TPU v7x, 32 devices: a whole 2x2x4 slice. The times are simulated.
32 devices in a mesh: sp: 8 (over z, y), tp: 4 (over x, core).
Axes of the slice: x: 2, y: 2, z: 4, core: 2. Of those that a mesh axis runs over, the one named last changes fastest.
Arguments:
- latent: bfloat16 [1024, 4096], P(('sp', 'tp')), may hold values from -8 to 8
- context: bfloat16 [256, 4096], P('sp'), may hold values from -6 to 6
- condition: float32 [4096], P('sp'), may hold values from -6 to 6
- context_condition: float32 [4096], P('sp'), may hold values from -6 to 6
- shift_weight: bfloat16 [4096, 4096], P('sp', 'tp'), may hold values from -0.09375 to 0.09375
- scale_weight: bfloat16 [4096, 4096], P('sp', 'tp'), may hold values from -0.09375 to 0.09375
- gate_weight: bfloat16 [4096, 4096], P('sp', 'tp'), may hold values from -0.09375 to 0.09375
- norm_gain: float32 [4096], replicated, may hold values from 0.1 to 1.9
- decay_down: bfloat16 [4096, 128], replicated, may hold values from -0.09375 to 0.09375
- decay_up: bfloat16 [128, 4096], P(None, 'tp'), may hold values from -0.5 to 0.5
- rate_down: bfloat16 [4096, 128], replicated, may hold values from -0.09375 to 0.09375
- rate_up: bfloat16 [128, 4096], P(None, 'tp'), may hold values from -0.5 to 0.5
- head_bias: float32 [2, 4096], P(None, 'tp'), may hold values from -12 to 1
- query_weight: bfloat16 [4096, 4096], P(None, 'tp'), may hold values from -0.09375 to 0.09375
- key_weight: bfloat16 [4096, 4096], P(None, 'tp'), may hold values from -0.09375 to 0.09375
- value_weight: bfloat16 [4096, 4096], P(None, 'tp'), may hold values from -0.09375 to 0.09375
- branch_weight: bfloat16 [4096, 4096], P(None, 'tp'), may hold values from -0.09375 to 0.09375
- group_gain: float32 [4096], P('tp'), may hold values from 0.1 to 1.9
- out_weight: bfloat16 [4096, 4096], P('tp'), may hold values from -0.09375 to 0.09375
Outputs:
- updated: bfloat16 [1024, 4096], P(('sp', 'tp'))
All inputs are finite; a program needn't handle non-finite values.
Results may differ from a plain program's by a relative error of at most 0.017.
Values may be sent and summed in bfloat16 or wider, within the bound.
A program may use at most 192 MiB of HBM per device.

v0:
```python
import functools
import math

import jax
import jax.numpy as jnp
from jax import lax
from jax.experimental import pallas as pl
from jax.experimental.pallas import tpu as pltpu
from jax.sharding import PartitionSpec as P

HEAD_DIM = 64
NORM_EPS = 1e-06
GROUP_EPS = 0.00064
DECAY_TOP = math.exp(-0.5)
BLOCK = 64
F32, BF16 = jnp.float32, jnp.bfloat16


def dot_dims(a, b, left, right):
    return lax.dot_general(
        a.astype(BF16), b.astype(BF16), (((left,), (right,)), ((), ())), preferred_element_type=F32
    )


def mm(a, b):
    return dot_dims(a, b, 1, 0)


def mmt(a, b):
    return dot_dims(a, b, 1, 1)


def tmm(a, b):
    return dot_dims(a, b, 0, 0)


def parts_of(x, count):
    found = []
    for _ in range(count):
        part = x.astype(BF16)
        found.append(part)
        x = x - part.astype(F32)
    return found


def head_ones(width):
    row = lax.broadcasted_iota(jnp.int32, (width, width), 0) // HEAD_DIM
    col = lax.broadcasted_iota(jnp.int32, (width, width), 1) // HEAD_DIM
    return (row == col).astype(F32)


def group_sum(x, ones, count=3):
    return sum(mm(part, ones) for part in parts_of(x, count))


def stack_heads(x):
    x = x.astype(BF16)
    count = x.shape[1] // HEAD_DIM
    if count == 1:
        return x
    lane = lax.broadcasted_iota(jnp.int32, (1, x.shape[1]), 1) // HEAD_DIM
    return jnp.concatenate([x * (lane == h).astype(F32).astype(BF16) for h in range(count)], axis=0)


def pack_heads(x):
    return sum(x[at : at + HEAD_DIM] for at in range(0, x.shape[0], HEAD_DIM))


def chain_inputs(keys, decay_pre, rate_pre, head_bias):
    k = keys.astype(F32)
    log_decay = -DECAY_TOP * jax.nn.sigmoid(head_bias[0:1] + decay_pre.astype(F32))
    rate = jax.nn.sigmoid(head_bias[1:2] + rate_pre.astype(F32))
    unit = k * lax.rsqrt(group_sum(k * k, head_ones(k.shape[1]), 2) + 1.0)
    return k, -unit, unit * rate, log_decay


def cumulate(log_decay, sign):
    row = lax.broadcasted_iota(jnp.int32, (BLOCK, BLOCK), 0)
    col = lax.broadcasted_iota(jnp.int32, (BLOCK, BLOCK), 1)
    mask = ((row - col) * sign >= 0).astype(F32)
    return sum(mm(mask, part) for part in parts_of(log_decay, 3))


def solve_blocks(items, width):
    row = lax.broadcasted_iota(jnp.int32, (BLOCK, width), 0)
    col = lax.broadcasted_iota(jnp.int32, (BLOCK, width), 1) % BLOCK
    ones = head_ones(width)
    square = lax.broadcasted_iota(jnp.int32, (width, width), 0)
    unit = (square == lax.broadcasted_iota(jnp.int32, (width, width), 1)).astype(F32)
    one = (row == col).astype(F32)
    work = []
    for sign, k, v, erase, write, log_decay, cum, q in items:
        strict = (row - col) * sign > 0
        inclusive = (row - col) * sign >= 0
        growth = jnp.exp(-cum)
        es = (erase * jnp.exp(cum - log_decay)).astype(BF16)
        right_w, right_k = stack_heads(write * growth), stack_heads(k * growth)
        item = {"es": es, "v": v.astype(BF16)}
        if q is not None:
            qs = q * jnp.exp(cum)
            left = jnp.concatenate([es, qs.astype(BF16)], axis=0)
        else:
            left = es
        by_w, by_k = mmt(left, right_w), mmt(left, right_k)
        item["coupling"] = jnp.where(strict, by_w[:BLOCK], 0.0)
        item["feed"] = jnp.where(strict, by_k[:BLOCK], 0.0)
        if q is not None:
            item["qs"] = qs
            item["aw"] = jnp.where(inclusive, by_w[BLOCK:], 0.0)
            item["ak"] = jnp.where(inclusive, by_k[BLOCK:], 0.0)
        if isinstance(sign, int):
            final = cum[BLOCK - 1 :] if sign > 0 else cum[0:1]
        else:
            final = jnp.where(sign > 0, cum[BLOCK - 1 :], cum[0:1])
        tail = jnp.exp(final - cum)
        item["wt"], item["kt"] = (write * tail).astype(BF16), (k * tail).astype(BF16)
        item["diagonal"] = unit * jnp.exp(final)
        work.append(item)
    near = (row // 2 == col // 2) & (row != col)
    for item in work:
        item["x"] = one + jnp.where(near, item["coupling"], 0.0)
        seen = stack_heads(item["v"])
        if "ak" in item:
            both = mm(jnp.concatenate([item["feed"], item["ak"]], axis=0), seen)
            item["fed"], item["akv"] = both[:BLOCK], both[BLOCK:]
        else:
            item["fed"] = mm(item["feed"], seen)
    size = 2
    while size < BLOCK:
        level = (row // (2 * size) == col // (2 * size)) & (row // size != col // size)
        for item in work:
            item["y"] = mm(jnp.where(level, item["coupling"], 0.0), stack_heads(item["x"]))
        for item in work:
            item["x"] = item["x"] + mm(item["x"], stack_heads(item["y"]))
        size *= 2
    for item in work:
        item["response"] = mm(item["x"], stack_heads(item["es"]))
        item["offset"] = mm(item["x"], stack_heads(item["fed"]))
    done = []
    for item in work:
        transfer = tmm(item["response"], item["wt"]) * ones + item["diagonal"]
        constant = (tmm(item["offset"], item["wt"]) + tmm(item["v"], item["kt"])) * ones
        if "aw" in item:
            query = item["qs"] + mm(item["aw"], stack_heads(item["response"]))
            base = item["akv"] + mm(item["aw"], stack_heads(item["offset"]))
            done.append((transfer, constant, query, base))
        else:
            done.append((transfer, constant, None, None))
    return done


def latent_kernel(width, q_ref, k_ref, v_ref, d_ref, r_ref, bias_ref, maps_ref, query_ref, base_ref):
    rows, lanes = k_ref.shape
    count = rows // BLOCK
    k, erase, write, log_decay = chain_inputs(k_ref[...], d_ref[...], r_ref[...], bias_ref[...])
    q, v = q_ref[...].astype(F32), v_ref[...]
    items, places = [], []
    for sign in (1, -1):
        for b in range(count):
            r = slice(b * BLOCK, (b + 1) * BLOCK)
            cum = cumulate(log_decay[r], sign)
            for p in range(lanes // width):
                c = slice(p * width, (p + 1) * width)
                items.append(
                    (sign, k[r, c], v[r, c], erase[r, c], write[r, c], log_decay[r, c], cum[:, c], q[r, c])
                )
                places.append((int(sign < 0), b, p))
    found = dict(zip(places, solve_blocks(items, width)))
    for p in range(lanes // width):
        c = slice(p * width, (p + 1) * width)
        bases = [None] * count
        for way in (0, 1):
            carried = None
            for b in (range(count) if way == 0 else reversed(range(count))):
                transfer, constant, query, base = found[(way, b, p)]
                if carried is not None:
                    base = base + mmt(query, carried[1])
                    query = mmt(query, carried[0])
                    transfer, constant = (
                        mm(carried[0], transfer),
                        mm(carried[1], transfer) + constant,
                    )
                carried = (transfer, constant)
                query_ref[way, b * BLOCK : (b + 1) * BLOCK, c] = query.astype(BF16)
                bases[b] = base if bases[b] is None else bases[b] + base
            maps_ref[way, p, 0] = pack_heads(carried[0]).astype(BF16)
            maps_ref[way, p, 1] = pack_heads(carried[1]).astype(BF16)
        for b in range(count):
            base_ref[b * BLOCK : (b + 1) * BLOCK, c] = bases[b]


def advance(state, transfer, constant):
    high, low = parts_of(state, 2)
    both = mm(jnp.concatenate([high, low], axis=0), transfer)
    return both[:HEAD_DIM] + both[HEAD_DIM:] + constant


def context_kernel(width, way_ref, features_ref, bias_ref, state_ref, transfers, constants):
    sources, _, rows, lanes = features_ref.shape
    way = way_ref[0]
    sign = 1 - 2 * way
    keys, v, decay_pre, rate_pre = (
        jnp.concatenate([features_ref[at, kind] for at in range(sources)], axis=0) for kind in range(4)
    )
    k, erase, write, log_decay = chain_inputs(keys, decay_pre, rate_pre, bias_ref[...])
    count = sources * rows // BLOCK
    items, places = [], []
    for b in range(count):
        r = slice(b * BLOCK, (b + 1) * BLOCK)
        cum = cumulate(log_decay[r], sign)
        for p in range(lanes // width):
            c = slice(p * width, (p + 1) * width)
            items.append(
                (sign, k[r, c], v[r, c], erase[r, c], write[r, c], log_decay[r, c], cum[:, c], None)
            )
            places.append((b, p))
    for (b, p), (transfer, constant, _, _) in zip(places, solve_blocks(items, width)):
        transfers[b, p] = transfer.astype(BF16)
        constants[b, p] = pack_heads(constant)
    packs = lanes // width
    states = [constants[jnp.where(way == 1, count - 1, 0), p] for p in range(packs)]
    for step in range(1, count):
        at = jnp.where(way == 1, count - 1 - step, step)
        for p in range(packs):
            states[p] = advance(states[p], transfers[at, p], constants[at, p])
    for p in range(packs):
        state_ref[p] = states[p]


def fold_kernel(way_ref, maps_ref, state_ref, entry_ref):
    count, packs = maps_ref.shape[:2]
    states = [state_ref[p] for p in range(packs)]
    way = way_ref[0]
    for step in range(count):
        at = jnp.where(way == 1, count - 1 - step, step)
        for p in range(packs):
            entry_ref[at, p] = states[p].astype(BF16)
        if step < count - 1:
            for p in range(packs):
                states[p] = advance(
                    states[p], stack_heads(maps_ref[at, p, 0]), maps_ref[at, p, 1].astype(F32)
                )


def read_kernel(width, query_ref, base_ref, entry_ref, branch_ref, gain_ref, mixed_ref):
    lanes = base_ref.shape[1]
    ones = head_ones(width)
    for p in range(lanes // width):
        c = slice(p * width, (p + 1) * width)
        reads = base_ref[:, c]
        for way in (0, 1):
            reads = reads + mmt(query_ref[way, :, c], stack_heads(entry_ref[way, p]))
        away = reads - group_sum(reads, ones) * (1.0 / HEAD_DIM)
        variance = group_sum(away * away, ones) * (1.0 / HEAD_DIM)
        branch = branch_ref[:, c].astype(F32)
        mixed_ref[:, c] = (
            away * lax.rsqrt(variance + GROUP_EPS) * gain_ref[:, c] * (branch * jax.nn.sigmoid(branch))
        ).astype(BF16)


def modulation_kernel(
    condition_ref, shift_ref, scale_ref, gate_ref, latent_ref, rows_ref, vectors_ref,
    parts, arrived, send_rows, take_rows, send_parts, take_parts, send_sum, take_sum,
):
    sp, tp = arrived.shape[0] + 1, rows_ref.shape[0]
    me_sp, me_tp = lax.axis_index("sp"), lax.axis_index("tp")
    barrier = pltpu.get_barrier_semaphore()
    for axis, me, size in (("sp", me_sp, sp), ("tp", me_tp, tp)):
        for d in range(1, size):
            pl.semaphore_signal(
                barrier, inc=1, device_id={axis: lax.rem(me + d, size)}, device_id_type=pl.DeviceIdType.MESH
            )
    pl.semaphore_wait(barrier, sp + tp - 2)

    def send(source, target, sent, taken, axis, peer):
        copy = pltpu.make_async_remote_copy(
            src_ref=source,
            dst_ref=target,
            send_sem=sent,
            recv_sem=taken,
            device_id={axis: peer},
            device_id_type=pl.DeviceIdType.MESH,
        )
        copy.start()
        return copy

    row_copies = [
        send(latent_ref, rows_ref.at[me_tp], send_rows.at[d - 1], take_rows.at[d - 1], "tp", lax.rem(me_tp + d, tp))
        for d in range(1, tp)
    ]
    values = condition_ref[...]
    conditions = (values * jax.nn.sigmoid(values)).astype(BF16)
    both = [mm(conditions, ref[...])[0:2] for ref in (shift_ref, scale_ref, gate_ref)]
    parts[...] = jnp.concatenate(both + [jnp.zeros_like(both[0])], axis=0)
    part_copies = [
        send(parts, arrived.at[d - 1], send_parts.at[d - 1], take_parts.at[d - 1], "sp", lax.rem(me_sp + d, sp))
        for d in range(1, sp)
    ]
    rows_ref[me_tp] = latent_ref[...]
    total = parts[...]
    for d in range(1, sp):
        part_copies[d - 1].wait_recv()
        total = total + arrived[d - 1]
    vectors_ref[me_tp] = total
    sum_copies = [
        send(vectors_ref.at[me_tp], vectors_ref.at[me_tp], send_sum.at[d - 1], take_sum.at[d - 1], "tp", lax.rem(me_tp + d, tp))
        for d in range(1, tp)
    ]
    for copy in part_copies:
        copy.wait_send()
    for copy in sum_copies + row_copies:
        copy.wait()


def modulated(rows, gain, scale, shift):
    values = rows.astype(F32)
    inverse = lax.rsqrt(jnp.mean(values * values, axis=-1, keepdims=True) + NORM_EPS)
    return (values * inverse * gain * (1.0 + scale) + shift).astype(BF16)


def project(rows, weight):
    return jnp.dot(rows, weight, preferred_element_type=F32).astype(BF16)


def summed_rows(shares):
    tp, me = lax.axis_size("tp"), lax.axis_index("tp")
    chips, core, chip = tp // 2, me % 2, me // 2
    blocks = shares.reshape(chips, 2, shares.shape[0] // tp, -1)
    mine = lax.dynamic_index_in_dim(blocks, core, 1, keepdims=False)
    other = lax.dynamic_index_in_dim(blocks, 1 - core, 1, keepdims=False)
    taken = lax.ppermute(other, "tp", [(at, at ^ 1) for at in range(tp)])
    both = mine.astype(F32) + taken.astype(F32)
    total = lax.dynamic_index_in_dim(both, chip, 0, keepdims=False)
    for d in range(1, chips):
        block = lax.dynamic_index_in_dim(both, (chip + d) % chips, 0, keepdims=False).astype(BF16)
        total = total + lax.ppermute(
            block, "tp", [(at, (at + 2 * d) % tp) for at in range(tp)]
        ).astype(F32)
    return total.astype(BF16).astype(F32)


def on_device(
    latent,
    context,
    condition,
    context_condition,
    shift_weight,
    scale_weight,
    gate_weight,
    norm_gain,
    decay_down,
    decay_up,
    rate_down,
    rate_up,
    head_bias,
    query_weight,
    key_weight,
    value_weight,
    branch_weight,
    group_gain,
    out_weight,
):
    local = query_weight.shape[1]
    devices, at_sp = lax.axis_size("sp"), lax.axis_index("sp")
    heads = local // HEAD_DIM
    joined = 2 if heads % devices == 0 else 1
    width = joined * HEAD_DIM
    packs = heads // joined
    own = 2 * packs // devices
    way = (at_sp * own) // packs
    first = (at_sp * own) % packs * width

    tp = lax.axis_size("tp")
    conditions = jnp.stack([condition, context_condition])
    conditions = jnp.pad(conditions, ((0, 6), (0, 0)))
    vmem = pl.BlockSpec(memory_space=pltpu.VMEM)
    rows_in, vectors = pl.pallas_call(
        modulation_kernel,
        in_specs=[vmem] * 5,
        out_specs=[vmem] * 2,
        out_shape=[
            jax.ShapeDtypeStruct((tp, *latent.shape), BF16),
            jax.ShapeDtypeStruct((tp, 8, local), F32),
        ],
        scratch_shapes=[
            pltpu.VMEM((8, local), F32),
            pltpu.VMEM((devices - 1, 8, local), F32),
            pltpu.SemaphoreType.DMA((tp - 1,)),
            pltpu.SemaphoreType.DMA((tp - 1,)),
            pltpu.SemaphoreType.DMA((devices - 1,)),
            pltpu.SemaphoreType.DMA((devices - 1,)),
            pltpu.SemaphoreType.DMA((tp - 1,)),
            pltpu.SemaphoreType.DMA((tp - 1,)),
        ],
        compiler_params=pltpu.CompilerParams(collective_id=0, has_side_effects=True),
        name="modulation",
    )(conditions, shift_weight, scale_weight, gate_weight, latent)
    rows_in = rows_in.reshape(-1, latent.shape[1])
    vectors = vectors.transpose(1, 0, 2).reshape(8, -1)
    shift, scale, gate = vectors[0:2], vectors[2:4], vectors[4]

    rows = rows_in.shape[0]
    normed = jnp.concatenate(
        [
            modulated(rows_in, norm_gain, scale[0], shift[0]),
            modulated(context, norm_gain, scale[1], shift[1]),
        ],
        axis=0,
    )
    decay_low = jnp.tanh(jnp.dot(normed, decay_down, preferred_element_type=F32)).astype(BF16)
    rate_low = project(normed, rate_down)
    keys, values = project(normed, key_weight), project(normed, value_weight)
    decay_pre, rate_pre = project(decay_low, decay_up), project(rate_low, rate_up)
    queries, branch = project(normed[:rows], query_weight), project(normed[:rows], branch_weight)
    features = jnp.stack([part[rows:] for part in (keys, values, decay_pre, rate_pre)])
    features = features.reshape(4, -1, packs // own, own * width).transpose(2, 0, 1, 3)
    features = lax.all_to_all(
        jnp.concatenate([features, features], axis=0), "sp", split_axis=0, concat_axis=0
    )

    group = min(2, packs)
    lanes = group * width
    tile = pl.BlockSpec((rows, lanes), lambda g: (0, g))
    maps, query, base = pl.pallas_call(
        functools.partial(latent_kernel, width),
        grid=(packs // group,),
        in_specs=[tile] * 5 + [pl.BlockSpec((2, lanes), lambda g: (0, g))],
        out_specs=[
            pl.BlockSpec((2, group, 2, HEAD_DIM, width), lambda g: (0, g, 0, 0, 0)),
            pl.BlockSpec((2, rows, lanes), lambda g: (0, 0, g)),
            tile,
        ],
        out_shape=[
            jax.ShapeDtypeStruct((2, packs, 2, HEAD_DIM, width), BF16),
            jax.ShapeDtypeStruct((2, rows, local), BF16),
            jax.ShapeDtypeStruct((rows, local), F32),
        ],
        name="latent_blocks",
    )(queries, keys, values, decay_pre, rate_pre, head_bias)

    count = features.shape[0] * features.shape[2] // BLOCK
    smem = pl.BlockSpec(memory_space=pltpu.SMEM)
    way = way.reshape(1).astype(jnp.int32)
    state = pl.pallas_call(
        functools.partial(context_kernel, width),
        in_specs=[smem, vmem, vmem],
        out_specs=vmem,
        out_shape=jax.ShapeDtypeStruct((own, HEAD_DIM, width), F32),
        scratch_shapes=[
            pltpu.VMEM((count, own, width, width), BF16),
            pltpu.VMEM((count, own, HEAD_DIM, width), F32),
        ],
        name="context_blocks",
    )(way, features, lax.dynamic_slice_in_dim(head_bias, first, own * width, axis=1))

    everyone = lax.all_to_all(
        maps.reshape(devices, own, 2, HEAD_DIM, width), "sp", split_axis=0, concat_axis=0
    )
    entries = pl.pallas_call(
        fold_kernel,
        in_specs=[smem, vmem, vmem],
        out_specs=vmem,
        out_shape=jax.ShapeDtypeStruct((devices, own, HEAD_DIM, width), BF16),
        name="fold_states",
    )(way, everyone, state)
    entry = lax.all_to_all(entries, "sp", split_axis=0, concat_axis=0)
    entry = entry.reshape(2, packs, HEAD_DIM, width)

    mixed = pl.pallas_call(
        functools.partial(read_kernel, width),
        out_shape=jax.ShapeDtypeStruct((rows, local), BF16),
        name="read_states",
    )(query, base, entry, branch, group_gain.reshape(1, local))

    mixer = jnp.concatenate(
        [
            summed_rows(jnp.dot(mixed, columns, preferred_element_type=F32).astype(BF16))
            for columns in jnp.split(out_weight, 2, axis=1)
        ],
        axis=1,
    )
    normed_out = mixer * lax.rsqrt(jnp.mean(mixer * mixer, axis=-1, keepdims=True) + NORM_EPS)
    return (latent.astype(F32) + gate * normed_out).astype(BF16)


def solution(mesh):
    placed = (
        P(("sp", "tp"), None),
        P("sp", None),
        P("sp"),
        P("sp"),
        P("sp", "tp"),
        P("sp", "tp"),
        P("sp", "tp"),
        P(),
        P(),
        P(None, "tp"),
        P(),
        P(None, "tp"),
        P(None, "tp"),
        P(None, "tp"),
        P(None, "tp"),
        P(None, "tp"),
        P(None, "tp"),
        P("tp"),
        P("tp", None),
    )
    return jax.shard_map(
        on_device, mesh=mesh, in_specs=placed, out_specs=P(("sp", "tp"), None), check_vma=False
    )
```

profile of v0, /device:TPU:0, one launch (start us, length us, event | category | flops | bytes accessed | tf_op | source)
XLA Modules:
  0.0 126.0 jit_solution(3043848472338845829)
XLA Ops:
  0.0 0.0 copy-start
  0.0 0.0 copy-start.11
  0.0 1.2 fusion.15
  1.2 1.3 %select_maximum_fusion.condition_ref = f32[8,512]{1,0:T(8,128)} fusion(f32[1,512]{1,0:T(1,128)} %bitcast.77, f32[1,512]{1,0:T(1,128)} %bitcast.78), kind=kLoop, calls=%fused_computation.52 | loop fusion | flops 16384 | bytes 20480 | tf_op jit(solution)/shard_map/stack | solution.py:374
  2.5 23.5 %modulation.1 = (bf16[4,32,4096]{2,1,0:T(8,128)(2,1)}, f32[4,8,1024]{2,1,0:T(8,128)}) custom-call(f32[8,512]{1,0:T(8,128)} %select_maximum_fusion.condition_ref, bf16[512,1024]{1,0:T(8,128)(2,1)} %shift_ref.1, bf16[512,1024]{1,0:T(8,128)(2,1)} %scale_ref.1, bf16[512,1024]{1,0:T(8,128)(2,1)} %gate_ref.1, bf16[32,4096]{1,0:T(8,128)(2,1)} %latent_ref.1), custom_call_target="tpu_custom_call" | custom-call | tf_op jit(solution)/shard_map/modulation/pallas_call | solution.py:377
  26.0 1.5 %fusion.28 = (f32[1,4,1024]{2,0,1:T(1,128)S(1)}, f32[1,4,1024]{2,0,1:T(1,128)S(1)}, f32[1,4,1024]{2,0,1:T(1,128)S(1)}, f32[1,4,1024]{2,0,1:T(1,128)S(1)}, f32[1,4,1024]{2,0,1:T(1,128)S(1)}) fusion(f32[8,4,1024]{2,0,1:T(8,128)} %bitcast.75), kind=kLoop, calls=%fused_computation.58 | loop fusion | flops 8192 | bytes 163840 | tf_op jit(solution)/shard_map/slice | solution.py:400
  27.5 1.5 %multiply_reduce_fusion = f32[4,32]{1,0:T(4,128)S(1)} fusion(bf16[4,32,4096]{2,1,0:T(8,128)(2,1)} %get-tuple-element.11), kind=kLoop, calls=%fused_computation.11 | loop fusion | flops 1572736 | bytes 1049088 | tf_op jit(solution)/shard_map/reduce_sum | solution.py:317
  29.0 0.1 rsqrt.28
  29.1 0.0 copy-done.11
  29.1 1.7 %fusion.13 = bf16[128,4096]{1,0:T(8,128)(2,1)S(1)} fusion(f32[4096]{0:T(1024)S(1)} %bitcast.70, f32[4096]{0:T(1024)S(1)} %bitcast.71, f32[4096]{0:T(1024)S(1)} %copy-done.11, f32[128]{0:T(128)S(1)} %rsqrt.28, bf16[4,32,4096]{2,1,0:T(8,128)(2,1)} %get-tuple-element.11), kind=kLoop, calls=%fused_computation.10 | loop fusion | flops 3145728 | bytes 2146816 | tf_op jit(solution)/shard_map/convert_element_type | solution.py:318
  30.8 0.0 copy-done.4
  30.8 0.2 fusion.19
  31.0 0.0 copy-start.12
  31.0 4.9 %convolution_convert_fusion.v_ref = bf16[160,1024]{1,0:T(8,128)(2,1)S(1)} fusion(bf16[4096,1024]{1,0:T(8,128)(2,1)} %param.34, bf16[32,4096]{1,0:T(8,128)(2,1)S(1)} %fusion.19, bf16[128,4096]{1,0:T(8,128)(2,1)S(1)} %fusion.13), kind=kOutput, calls=%fused_computation.13 | convolution fusion | flops 1344962560 | bytes 10027008 | tf_op jit(solution)/shard_map/dot_general | solution.py:322
  35.9 0.0 copy-start.6
  36.0 0.0 copy-done
  36.0 0.0 copy-done.12
  36.0 0.7 convolution_convert_fusion.3.d_ref
  36.7 0.0 copy-start.7
  36.8 0.0 copy-start.13
  36.8 5.0 %convolution_convert_fusion.1.k_ref = bf16[160,1024]{1,0:T(8,128)(2,1)S(1)} fusion(bf16[4096,1024]{1,0:T(8,128)(2,1)} %param.33, bf16[32,4096]{1,0:T(8,128)(2,1)S(1)} %fusion.19, bf16[128,4096]{1,0:T(8,128)(2,1)S(1)} %fusion.13), kind=kOutput, calls=%fused_computation.14 | convolution fusion | flops 1344962560 | bytes 10027008 | tf_op jit(solution)/shard_map/dot_general | solution.py:322
  41.8 0.0 copy-done.6
  41.8 0.0 copy-done.7
  41.8 0.0 copy-start.8
  41.8 0.7 copy-done.8
  42.6 0.0 copy-done.13
  42.6 1.9 %convolution_convert_fusion.2.r_ref = bf16[160,1024]{1,0:T(8,128)(2,1)S(1)} fusion(bf16[128,1024]{1,0:T(8,128)(2,1)S(1)} %copy-done.13, bf16[4096,128]{1,0:T(8,128)(2,1)} %param.29, bf16[32,4096]{1,0:T(8,128)(2,1)S(1)} %fusion.19, bf16[128,4096]{1,0:T(8,128)(2,1)S(1)} %fusion.13), kind=kOutput, calls=%fused_computation.15 | convolution fusion | flops 212520960 | bytes 2949120 | tf_op jit(solution)/shard_map/dot_general | solution.py:322
  44.5 0.0 copy-start.9
  44.6 0.9 pad_maximum_fusion.1
  45.5 3.5 %all-to-all-start.1 = ((bf16[8,4,32,256]{3,2,1,0:T(8,128)(2,1)}), bf16[8,4,32,256]{3,2,1,0:T(8,128)(2,1)S(1)}, u32[]{:S(2)}, u32[]{:S(2)}) async-start(bf16[8,4,32,256]{3,2,1,0:T(8,128)(2,1)} %pad_maximum_fusion.1), calls=%async_computation.1 | async-start | bytes 1048576 | tf_op jit(solution)/shard_map/all_to_all | solution.py:417
  49.0 5.3 %convolution_convert_fusion.5.q_ref = bf16[128,1024]{1,0:T(8,128)(2,1)} fusion(bf16[128,4096]{1,0:T(8,128)(2,1)S(1)} %fusion.13, bf16[4096,1024]{1,0:T(8,128)(2,1)} %param.32), kind=kOutput, calls=%fused_computation.18 | convolution fusion | flops 1073872896 | bytes 9699328 | tf_op jit(solution)/shard_map/dot_general | solution.py:322
  54.3 0.0 copy-done.9
  54.3 13.7 %latent_blocks.1 = (bf16[2,8,2,64,128]{4,3,2,1,0:T(8,128)(2,1)}, bf16[2,128,1024]{2,1,0:T(8,128)(2,1)}, f32[128,1024]{1,0:T(8,128)}) custom-call(bf16[128,1024]{1,0:T(8,128)(2,1)} %convolution_convert_fusion.5.q_ref, bf16[160,1024]{1,0:T(8,128)(2,1)} %copy-done.8, bf16[160,1024]{1,0:T(8,128)(2,1)} %copy-done.6, bf16[160,1024]{1,0:T(8,128)(2,1)} %copy-done.7, ...), custom_call_target="tpu_custom_call" | custom-call | tf_op jit(solution)/shard_map/latent_blocks/pallas_call | solution.py:424
  68.0 0.0 all-to-all-done.1.features_ref
  68.0 0.0 copy-start.1
  68.1 5.9 %all-to-all-start = ((bf16[8,2,2,64,128]{4,3,2,1,0:T(8,128)(2,1)}), bf16[8,2,2,64,128]{4,3,2,1,0:T(8,128)(2,1)S(1)}, u32[]{:S(2)}, u32[]{:S(2)}) async-start(bf16[8,2,2,64,128]{4,3,2,1,0:T(8,128)(2,1)} %bitcast.65), calls=%async_computation | async-start | bytes 1048576 | tf_op jit(solution)/shard_map/all_to_all | solution.py:456
  74.0 1.3 constant_dynamic-slice_fusion.bias_ref
  75.3 0.0 copy-done.1
  75.3 4.7 %context_blocks.1.state_ref = f32[2,64,128]{2,1,0:T(8,128)} custom-call(s32[1]{0:T(128)} %bitcast.9.way_ref, bf16[8,4,32,256]{3,2,1,0:T(8,128)(2,1)} %copy-done.1, f32[2,256]{1,0:T(2,128)} %constant_dynamic-slice_fusion.bias_ref), custom_call_target="tpu_custom_call" | custom-call | tf_op jit(solution)/shard_map/context_blocks/pallas_call | solution.py:444
  80.0 8.5 %all-to-all-done.maps_ref = bf16[8,2,2,64,128]{4,3,2,1,0:T(8,128)(2,1)S(1)} async-done(((bf16[8,2,2,64,128]{4,3,2,1,0:T(8,128)(2,1)}), bf16[8,2,2,64,128]{4,3,2,1,0:T(8,128)(2,1)S(1)}, u32[]{:S(2)}, u32[]{:S(2)}) %all-to-all-start) | async-done | bytes 524320 | tf_op jit(solution)/shard_map/all_to_all | solution.py:456
  88.6 0.8 copy-done.2
  89.4 2.7 %fold_states.1 = bf16[8,2,64,128]{3,2,1,0:T(8,128)(2,1)} custom-call(s32[1]{0:T(128)} %bitcast.9.way_ref, bf16[8,2,2,64,128]{4,3,2,1,0:T(8,128)(2,1)} %copy-done.2, f32[2,64,128]{2,1,0:T(8,128)} %context_blocks.1.state_ref), custom_call_target="tpu_custom_call" | custom-call | tf_op jit(solution)/shard_map/fold_states/pallas_call | solution.py:459
  92.1 3.6 %all-to-all-start.2 = ((bf16[8,2,64,128]{3,2,1,0:T(8,128)(2,1)}), bf16[8,2,64,128]{3,2,1,0:T(8,128)(2,1)S(1)}, u32[]{:S(2)}, u32[]{:S(2)}) async-start(bf16[8,2,64,128]{3,2,1,0:T(8,128)(2,1)} %fold_states.1), calls=%async_computation.2 | async-start | bytes 524288 | tf_op jit(solution)/shard_map/all_to_all | solution.py:466
  95.8 5.3 %convolution_convert_fusion.4.branch_ref = bf16[128,1024]{1,0:T(8,128)(2,1)} fusion(bf16[128,4096]{1,0:T(8,128)(2,1)S(1)} %fusion.13, bf16[4096,1024]{1,0:T(8,128)(2,1)} %param.35), kind=kOutput, calls=%fused_computation.17 | convolution fusion | flops 1073872896 | bytes 9699328 | tf_op jit(solution)/shard_map/dot_general | solution.py:322
  101.1 3.8 %all-to-all-done.2 = bf16[8,2,64,128]{3,2,1,0:T(8,128)(2,1)S(1)} async-done(((bf16[8,2,64,128]{3,2,1,0:T(8,128)(2,1)}), bf16[8,2,64,128]{3,2,1,0:T(8,128)(2,1)S(1)}, u32[]{:S(2)}, u32[]{:S(2)}) %all-to-all-start.2) | async-done | bytes 262176 | tf_op jit(solution)/shard_map/all_to_all | solution.py:466
  104.9 0.7 copy-done.3
  105.6 4.3 %read_states.1 = bf16[128,1024]{1,0:T(8,128)(2,1)} custom-call(bf16[2,128,1024]{2,1,0:T(8,128)(2,1)} %get-tuple-element.12.query_ref, f32[128,1024]{1,0:T(8,128)} %get-tuple-element.13.base_ref, bf16[2,8,64,128]{3,2,1,0:T(8,128)(2,1)} %bitcast.64, bf16[128,1024]{1,0:T(8,128)(2,1)} %convolution_convert_fusion.4.branch_ref, f32[1,1024]{1,0:T(1,128)} %bitcast.76), custom_call_target="tpu_custom_call" | custom-call | tf_op jit(solution)/shard_map/read_states/pallas_call | solution.py:469
  109.9 3.0 %fusion.4 = bf16[128,2048]{1,0:T(8,128)(2,1)S(1)} fusion(bf16[128,1024]{1,0:T(8,128)(2,1)} %read_states.1, bf16[1024,4096]{1,0:T(8,128)(2,1)} %param.37), kind=kOutput, calls=%fused_computation.4 | convolution fusion | flops 537133056 | bytes 4980736 | tf_op jit(solution)/shard_map/dot_general | solution.py:477
  112.9 0.1 collective-permute-start
  113.0 0.0 copy-done.10
  113.0 2.9 %fusion.7 = bf16[128,2048]{1,0:T(8,128)(2,1)S(1)} fusion(bf16[128,1024]{1,0:T(8,128)(2,1)S(1)} %copy-done.10, bf16[1024,4096]{1,0:T(8,128)(2,1)} %param.37), kind=kOutput, calls=%fused_computation.5 | convolution fusion | flops 537133056 | bytes 4980736 | tf_op jit(solution)/shard_map/dot_general | solution.py:477
  115.9 0.0 copy-start.5
  116.0 0.5 collective-permute-start.2
  116.5 0.0 collective-permute-done
  116.5 0.1 convert_add_fusion.1
  116.6 0.6 collective-permute-start.1
  117.2 0.5 collective-permute-done.2
  117.7 0.1 convert_add_fusion
  117.8 1.1 collective-permute-start.3
  118.9 4.2 %collective-permute-done.1 = bf16[32,2048]{1,0:T(8,128)(2,1)S(1)} collective-permute-done((bf16[32,2048]{1,0:T(8,128)(2,1)S(1)}, bf16[32,2048]{1,0:T(8,128)(2,1)S(1)}, u32[]{:S(2)}, u32[]{:S(2)}) %collective-permute-start.1) | collective-permute-done | bytes 131104 | tf_op jit(solution)/shard_map/ppermute | solution.py:336
  123.1 1.8 %collective-permute-done.3 = bf16[32,2048]{1,0:T(8,128)(2,1)S(1)} collective-permute-done((bf16[32,2048]{1,0:T(8,128)(2,1)S(1)}, bf16[32,2048]{1,0:T(8,128)(2,1)S(1)}, u32[]{:S(2)}, u32[]{:S(2)}) %collective-permute-start.3) | collective-permute-done | bytes 131104 | tf_op jit(solution)/shard_map/ppermute | solution.py:336
  125.0 0.2 fusion.20
  125.1 0.0 copy-done.5
  125.1 0.9 fusion.23
  (26 shorter events, 0.4 us)
Async XLA Ops:
  0.0 36.0 %copy-start = (bf16[4096,128]{1,0:T(8,128)(2,1)S(1)}, bf16[4096,128]{1,0:T(8,128)(2,1)}, u32[]{:S(2)}) copy-start(bf16[4096,128]{1,0:T(8,128)(2,1)} %param.27) | copy-start | bytes 3145732
  0.0 29.1 %copy-start.11 = (f32[4096]{0:T(1024)S(1)}, f32[4096]{0:T(1024)}, u32[]{:S(2)}) copy-start(f32[4096]{0:T(1024)} %param.26) | copy-start | bytes 49156
  2.5 28.2 %copy-start.4 = (bf16[32,4096]{1,0:T(8,128)(2,1)S(1)}, bf16[32,4096]{1,0:T(8,128)(2,1)}, u32[]{:S(2)}) copy-start(bf16[32,4096]{1,0:T(8,128)(2,1)} %param.20) | copy-start | bytes 786436
  31.0 5.1 %copy-start.12 = (bf16[128,1024]{1,0:T(8,128)(2,1)S(1)}, bf16[128,1024]{1,0:T(8,128)(2,1)}, u32[]{:S(2)}) copy-start(bf16[128,1024]{1,0:T(8,128)(2,1)} %param.28) | copy-start | bytes 786436
  35.9 5.9 %copy-start.6 = (bf16[160,1024]{1,0:T(8,128)(2,1)}, bf16[160,1024]{1,0:T(8,128)(2,1)S(1)}, u32[]{:S(2)}) copy-start(bf16[160,1024]{1,0:T(8,128)(2,1)S(1)} %convolution_convert_fusion.v_ref) | copy-start | bytes 983044
  36.7 5.1 %copy-start.7 = (bf16[160,1024]{1,0:T(8,128)(2,1)}, bf16[160,1024]{1,0:T(8,128)(2,1)S(1)}, u32[]{:S(2)}) copy-start(bf16[160,1024]{1,0:T(8,128)(2,1)S(1)} %convolution_convert_fusion.3.d_ref) | copy-start | bytes 983044
  36.8 5.8 %copy-start.13 = (bf16[128,1024]{1,0:T(8,128)(2,1)S(1)}, bf16[128,1024]{1,0:T(8,128)(2,1)}, u32[]{:S(2)}) copy-start(bf16[128,1024]{1,0:T(8,128)(2,1)} %param.30) | copy-start | bytes 786436
  41.8 0.7 copy-start.8
  44.5 9.8 %copy-start.9 = (bf16[160,1024]{1,0:T(8,128)(2,1)}, bf16[160,1024]{1,0:T(8,128)(2,1)S(1)}, u32[]{:S(2)}) copy-start(bf16[160,1024]{1,0:T(8,128)(2,1)S(1)} %convolution_convert_fusion.2.r_ref) | copy-start | bytes 983044
  45.5 22.6 %all-to-all-start.1 = ((bf16[8,4,32,256]{3,2,1,0:T(8,128)(2,1)}), bf16[8,4,32,256]{3,2,1,0:T(8,128)(2,1)S(1)}, u32[]{:S(2)}, u32[]{:S(2)}) async-start(bf16[8,4,32,256]{3,2,1,0:T(8,128)(2,1)} %pad_maximum_fusion.1), calls=%async_computation.1 | async-start | bytes 1048576 | tf_op jit(solution)/shard_map/all_to_all | solution.py:417
  68.0 7.2 %copy-start.1 = (bf16[8,4,32,256]{3,2,1,0:T(8,128)(2,1)}, bf16[8,4,32,256]{3,2,1,0:T(8,128)(2,1)S(1)}, u32[]{:S(2)}) copy-start(bf16[8,4,32,256]{3,2,1,0:T(8,128)(2,1)S(1)} %all-to-all-done.1.features_ref) | copy-start | bytes 1572868
  68.1 20.5 %all-to-all-start = ((bf16[8,2,2,64,128]{4,3,2,1,0:T(8,128)(2,1)}), bf16[8,2,2,64,128]{4,3,2,1,0:T(8,128)(2,1)S(1)}, u32[]{:S(2)}, u32[]{:S(2)}) async-start(bf16[8,2,2,64,128]{4,3,2,1,0:T(8,128)(2,1)} %bitcast.65), calls=%async_computation | async-start | bytes 1048576 | tf_op jit(solution)/shard_map/all_to_all | solution.py:456
  88.6 0.8 copy-start.2
  92.1 12.7 %all-to-all-start.2 = ((bf16[8,2,64,128]{3,2,1,0:T(8,128)(2,1)}), bf16[8,2,64,128]{3,2,1,0:T(8,128)(2,1)S(1)}, u32[]{:S(2)}, u32[]{:S(2)}) async-start(bf16[8,2,64,128]{3,2,1,0:T(8,128)(2,1)} %fold_states.1), calls=%async_computation.2 | async-start | bytes 524288 | tf_op jit(solution)/shard_map/all_to_all | solution.py:466
  104.8 0.7 copy-start.3
  109.9 3.2 %copy-start.10 = (bf16[128,1024]{1,0:T(8,128)(2,1)S(1)}, bf16[128,1024]{1,0:T(8,128)(2,1)}, u32[]{:S(2)}) copy-start(bf16[128,1024]{1,0:T(8,128)(2,1)} %read_states.1) | copy-start | bytes 786436
  112.9 3.6 %collective-permute-start = (bf16[2,32,2048]{2,1,0:T(8,128)(2,1)S(1)}, bf16[2,32,2048]{2,1,0:T(8,128)(2,1)S(1)}, u32[]{:S(2)}, u32[]{:S(2)}) collective-permute-start(bf16[2,32,2048]{2,1,0:T(8,128)(2,1)S(1)} %dynamic-slice_bitcast_fusion.1), channel_id=1, source_target_pairs={{0,1},{1,0},{2,3},{3,2},{4,5},{5,4},{6,7},{7,6},{8,9},{9,8},{10,11... | collective-permute-start | bytes 786440 | tf_op jit(solution)/shard_map/ppermute | solution.py:331
  115.9 9.2 %copy-start.5 = (bf16[32,4096]{1,0:T(8,128)(2,1)S(1)}, bf16[32,4096]{1,0:T(8,128)(2,1)}, u32[]{:S(2)}) copy-start(bf16[32,4096]{1,0:T(8,128)(2,1)} %latent_ref.1) | copy-start | bytes 786436
  116.0 1.7 %collective-permute-start.2 = (bf16[2,32,2048]{2,1,0:T(8,128)(2,1)S(1)}, bf16[2,32,2048]{2,1,0:T(8,128)(2,1)S(1)}, u32[]{:S(2)}, u32[]{:S(2)}) collective-permute-start(bf16[2,32,2048]{2,1,0:T(8,128)(2,1)S(1)} %dynamic-slice_bitcast_fusion), channel_id=1, source_target_pairs={{0,1},{1,0},{2,3},{3,2},{4,5},{5,4},{6,7},{7,6},{8,9},{9,8},{10,11... | collective-permute-start | bytes 786440 | tf_op jit(solution)/shard_map/ppermute | solution.py:331
  116.6 6.4 %collective-permute-start.1 = (bf16[32,2048]{1,0:T(8,128)(2,1)S(1)}, bf16[32,2048]{1,0:T(8,128)(2,1)S(1)}, u32[]{:S(2)}, u32[]{:S(2)}) collective-permute-start(bf16[32,2048]{1,0:T(8,128)(2,1)S(1)} %fusion.26), channel_id=1, source_target_pairs={{0,2},{1,3},{2,0},{3,1},{4,6},{5,7},{6,4},{7,5},{8,10},{9,11},{10,... | collective-permute-start | bytes 393224 | tf_op jit(solution)/shard_map/ppermute | solution.py:336
  117.8 7.1 %collective-permute-start.3 = (bf16[32,2048]{1,0:T(8,128)(2,1)S(1)}, bf16[32,2048]{1,0:T(8,128)(2,1)S(1)}, u32[]{:S(2)}, u32[]{:S(2)}) collective-permute-start(bf16[32,2048]{1,0:T(8,128)(2,1)S(1)} %fusion.27), channel_id=1, source_target_pairs={{0,2},{1,3},{2,0},{3,1},{4,6},{5,7},{6,4},{7,5},{8,10},{9,11},{10,... | collective-permute-start | bytes 393224 | tf_op jit(solution)/shard_map/ppermute | solution.py:336
where the time goes:
time: 127 us; the launch traced here: 126 us
  Pallas kernels  49 us (39%)
  matrix products  29.1 us (23%)
  waiting for transfers between devices  18.8 us (15%)
  starting transfers between devices  15.4 us (12%)
  other arithmetic  9.46 us (7%)
  local copies, waits for them, and re-layouts  3.94 us (3%)
    pallas_call x1, Pallas kernels, on_device(): pl.pallas_call(modulation_kernel, in_specs=[vmem] * 5, out_specs=[vmem] *...  23.5 us
    dot_general x6, matrix products, project(): return jnp.dot(rows, weight, preferred_element_type=F32).astype(BF16)  23.2 us
    pallas_call x1, Pallas kernels, on_device(): pl.pallas_call(functools.partial(latent_kernel, width), grid=(packs // gr...  13.7 us
    all_to_all x1, waiting for transfers between devices, on_device(): lax.all_to_all(maps.reshape(devices, own, 2, HEAD_DIM, width), 'sp', spli...  8.54 us
    ppermute x2, waiting for transfers between devices, summed_rows(): lax.ppermute(block, 'tp', [(at, (at + 2 * d) % tp) for at in range(tp)])  6.02 us
    all_to_all x1, starting transfers between devices, on_device(): lax.all_to_all(maps.reshape(devices, own, 2, HEAD_DIM, width), 'sp', spli...  5.95 us
    dot_general x2, matrix products, on_device(): jnp.dot(mixed, columns, preferred_element_type=F32).astype(BF16)  5.94 us
    pallas_call x1, Pallas kernels, on_device(): pl.pallas_call(functools.partial(context_kernel, width), in_specs=[smem,...  4.74 us
  transfers between devices with their start and end apart: 7, of which 5 were waited for; matrix products, arithmetic and copies ran while one was open for 12% of the time, Pallas kernels for 15%

commit v1 on v0

v1 whole, which is shorter than its diff:
```python
import functools
import math

import jax
import jax.numpy as jnp
from jax import lax
from jax.experimental import pallas as pl
from jax.experimental.pallas import tpu as pltpu
from jax.sharding import PartitionSpec as P

HEAD_DIM = 64
NORM_EPS = 1e-06
GROUP_EPS = 0.00064
DECAY_TOP = math.exp(-0.5)
BLOCK = 64
F32, BF16 = jnp.float32, jnp.bfloat16


def dot_dims(a, b, left, right):
    return lax.dot_general(
        a.astype(BF16), b.astype(BF16), (((left,), (right,)), ((), ())), preferred_element_type=F32
    )


def mm(a, b):
    return dot_dims(a, b, 1, 0)


def mmt(a, b):
    return dot_dims(a, b, 1, 1)


def tmm(a, b):
    return dot_dims(a, b, 0, 0)


def parts_of(x, count):
    found = []
    for _ in range(count):
        part = x.astype(BF16)
        found.append(part)
        x = x - part.astype(F32)
    return found


def head_ones(width):
    row = lax.broadcasted_iota(jnp.int32, (width, width), 0) // HEAD_DIM
    col = lax.broadcasted_iota(jnp.int32, (width, width), 1) // HEAD_DIM
    return (row == col).astype(F32)


def group_sum(x, ones, count=3):
    return sum(mm(part, ones) for part in parts_of(x, count))


def stack_heads(x):
    x = x.astype(BF16)
    count = x.shape[1] // HEAD_DIM
    if count == 1:
        return x
    lane = lax.broadcasted_iota(jnp.int32, (1, x.shape[1]), 1) // HEAD_DIM
    return jnp.concatenate([x * (lane == h).astype(F32).astype(BF16) for h in range(count)], axis=0)


def pack_heads(x):
    return sum(x[at : at + HEAD_DIM] for at in range(0, x.shape[0], HEAD_DIM))


def chain_inputs(keys, decay_pre, rate_pre, head_bias):
    k = keys.astype(F32)
    log_decay = -DECAY_TOP * jax.nn.sigmoid(head_bias[0:1] + decay_pre.astype(F32))
    rate = jax.nn.sigmoid(head_bias[1:2] + rate_pre.astype(F32))
    unit = k * lax.rsqrt(group_sum(k * k, head_ones(k.shape[1]), 2) + 1.0)
    return k, -unit, unit * rate, log_decay


def cumulate(log_decay, sign):
    row = lax.broadcasted_iota(jnp.int32, (BLOCK, BLOCK), 0)
    col = lax.broadcasted_iota(jnp.int32, (BLOCK, BLOCK), 1)
    mask = ((row - col) * sign >= 0).astype(F32)
    return sum(mm(mask, part) for part in parts_of(log_decay, 3))


def solve_blocks(items, width):
    row = lax.broadcasted_iota(jnp.int32, (BLOCK, width), 0)
    col = lax.broadcasted_iota(jnp.int32, (BLOCK, width), 1) % BLOCK
    ones = head_ones(width)
    square = lax.broadcasted_iota(jnp.int32, (width, width), 0)
    unit = (square == lax.broadcasted_iota(jnp.int32, (width, width), 1)).astype(F32)
    one = (row == col).astype(F32)
    work = []
    for sign, k, v, erase, write, log_decay, cum, q in items:
        strict = (row - col) * sign > 0
        inclusive = (row - col) * sign >= 0
        growth = jnp.exp(-cum)
        es = (erase * jnp.exp(cum - log_decay)).astype(BF16)
        right_w, right_k = stack_heads(write * growth), stack_heads(k * growth)
        item = {"es": es, "v": v.astype(BF16)}
        if q is not None:
            qs = q * jnp.exp(cum)
            left = jnp.concatenate([es, qs.astype(BF16)], axis=0)
        else:
            left = es
        by_w, by_k = mmt(left, right_w), mmt(left, right_k)
        item["coupling"] = jnp.where(strict, by_w[:BLOCK], 0.0)
        item["feed"] = jnp.where(strict, by_k[:BLOCK], 0.0)
        if q is not None:
            item["qs"] = qs
            item["aw"] = jnp.where(inclusive, by_w[BLOCK:], 0.0)
            item["ak"] = jnp.where(inclusive, by_k[BLOCK:], 0.0)
        if isinstance(sign, int):
            final = cum[BLOCK - 1 :] if sign > 0 else cum[0:1]
        else:
            final = jnp.where(sign > 0, cum[BLOCK - 1 :], cum[0:1])
        tail = jnp.exp(final - cum)
        item["wt"], item["kt"] = (write * tail).astype(BF16), (k * tail).astype(BF16)
        item["diagonal"] = unit * jnp.exp(final)
        work.append(item)
    near = (row // 2 == col // 2) & (row != col)
    for item in work:
        item["x"] = one + jnp.where(near, item["coupling"], 0.0)
        seen = stack_heads(item["v"])
        if "ak" in item:
            both = mm(jnp.concatenate([item["feed"], item["ak"]], axis=0), seen)
            item["fed"], item["akv"] = both[:BLOCK], both[BLOCK:]
        else:
            item["fed"] = mm(item["feed"], seen)
    size = 2
    while size < BLOCK:
        level = (row // (2 * size) == col // (2 * size)) & (row // size != col // size)
        for item in work:
            item["y"] = mm(jnp.where(level, item["coupling"], 0.0), stack_heads(item["x"]))
        for item in work:
            item["x"] = item["x"] + mm(item["x"], stack_heads(item["y"]))
        size *= 2
    for item in work:
        item["response"] = mm(item["x"], stack_heads(item["es"]))
        item["offset"] = mm(item["x"], stack_heads(item["fed"]))
    done = []
    for item in work:
        transfer = tmm(item["response"], item["wt"]) * ones + item["diagonal"]
        constant = (tmm(item["offset"], item["wt"]) + tmm(item["v"], item["kt"])) * ones
        if "aw" in item:
            query = item["qs"] + mm(item["aw"], stack_heads(item["response"]))
            base = item["akv"] + mm(item["aw"], stack_heads(item["offset"]))
            done.append((transfer, constant, query, base))
        else:
            done.append((transfer, constant, None, None))
    return done


MESH = pl.DeviceIdType.MESH


def solve_pack(k, v, erase, write, log_decay, q, signs):
    items = []
    for sign in signs:
        for at in range(0, k.shape[0], BLOCK):
            r = slice(at, at + BLOCK)
            cum = cumulate(log_decay[r], sign)
            items.append(
                (sign, k[r], v[r], erase[r], write[r], log_decay[r], cum, None if q is None else q[r])
            )
    return items


def advance(state, transfer, constant):
    high, low = parts_of(state, 2)
    both = mm(jnp.concatenate([high, low], axis=0), transfer)
    return both[:HEAD_DIM] + both[HEAD_DIM:] + constant


class Plan:
    def __init__(self, sp, tp, rows, context_rows, depth, local):
        self.sp, self.tp, self.chips = sp, tp, tp // 2
        self.block, self.context_rows = rows, context_rows
        self.rows = rows * tp
        self.depth, self.local = depth, local
        heads = local // HEAD_DIM
        self.width = (2 if heads % sp == 0 else 1) * HEAD_DIM
        self.packs = local // self.width
        self.units = 2 * self.packs // sp
        assert self.units in (1, 2) and self.units * sp == 2 * self.packs
        self.chunk = max(128, local // sp)
        self.owners = local // self.chunk
        self.tile = 512
        self.out_tile = 1024
        self.out_tiles = depth // self.out_tile
        self.context_blocks = context_rows * sp // BLOCK


def remote(source, target, sent, taken, **peer):
    return pltpu.make_async_remote_copy(
        src_ref=source,
        dst_ref=target,
        send_sem=sent,
        recv_sem=taken,
        device_id=peer,
        device_id_type=MESH,
    )


def layer_kernel(
    plan,
    latent_hbm, context_hbm, condition_ref, context_condition_ref,
    shift_hbm, scale_hbm, gate_hbm, norm_gain_ref,
    decay_down_hbm, decay_up_hbm, rate_down_hbm, rate_up_hbm, bias_ref,
    query_hbm, key_hbm, value_hbm, branch_hbm, group_gain_ref, out_hbm,
    updated_ref,
    rows_v, context_v, wmod_v, wdown_v, wup_v, wbig_v, wout_v,
    parts_v, part_in_v, vectors_v, mod_v, gate_v, inverse_v, normed_v,
    key_v, value_v, decay_v, rate_v, query_v, branch_v, bias_v,
    feature_out_v, feature_in_v, maps_out_v, maps_in_v, reads_q_v, base_v,
    transfer_v, constant_v, entry_out_v, entry_in_v, mixed_v,
    partial_v, pair_v, cross_out_v, cross_in_v, mixer_v,
    local_sem, row_s, row_r, relay_s, relay_r, part_s, part_r, vec_s, vec_r,
    feat_s, feat_r, map_s, map_r, ent_s, ent_r, pair_s, pair_r, cross_s, cross_r,
):
    sp, tp, chips, width, packs, units = plan.sp, plan.tp, plan.chips, plan.width, plan.packs, plan.units
    depth, local, block = plan.depth, plan.local, plan.block
    me_sp, me_tp = lax.axis_index("sp"), lax.axis_index("tp")
    chip, core = me_tp // 2, lax.rem(me_tp, 2)
    sibling = chip * 2 + 1 - core

    fetches = {}

    def fetch(name, at, source, target):
        copy = pltpu.make_async_copy(source, target, local_sem.at[at])
        copy.start()
        fetches[name] = copy

    fetch("shift", 0, shift_hbm, wmod_v.at[0])
    fetch("scale", 1, scale_hbm, wmod_v.at[1])
    fetch("gate", 2, gate_hbm, wmod_v.at[2])
    fetch("latent", 3, latent_hbm, rows_v.at[me_tp])
    fetch("context", 4, context_hbm, context_v)

    barrier = pltpu.get_barrier_semaphore()
    everyone = [(a, b) for a in range(sp) for b in range(tp) if (a, b) != (0, 0)]
    for a, b in everyone:
        pl.semaphore_signal(
            barrier,
            inc=1,
            device_id={"sp": lax.rem(me_sp + a, sp), "tp": lax.rem(me_tp + b, tp)},
            device_id_type=MESH,
        )

    fetch("decay_down", 5, decay_down_hbm, wdown_v.at[:, 0 : decay_down_hbm.shape[1]])
    fetch("rate_down", 6, rate_down_hbm, wdown_v.at[:, decay_down_hbm.shape[1] :])
    line = lax.broadcasted_iota(jnp.int32, (8, condition_ref.shape[1]), 0)
    values = jnp.where(line == 0, condition_ref[...], jnp.where(line == 1, context_condition_ref[...], 0.0))
    conditions = (values * jax.nn.sigmoid(values)).astype(BF16)
    shares = []
    for at, name in enumerate(("shift", "scale", "gate")):
        fetches[name].wait()
        shares.append(mm(conditions, wmod_v[at])[0:2])
    fetch("key", 7, key_hbm, wbig_v.at[0])
    fetch("value", 8, value_hbm, wbig_v.at[1])
    shares = jnp.concatenate(shares + [jnp.zeros_like(shares[0])], axis=0)
    for j in range(plan.owners):
        parts_v[j] = shares[:, j * plan.chunk : (j + 1) * plan.chunk]

    pl.semaphore_wait(barrier, len(everyone))

    def part_copy(d):
        peer = lax.rem(me_sp + d, sp)
        return peer, remote(
            parts_v.at[peer], part_in_v.at[d - 1], part_s.at[d - 1], part_r.at[d - 1], sp=peer, tp=me_tp
        )

    def when_owner(at, body):
        if plan.owners == sp:
            body()
        else:
            pl.when(at < plan.owners)(body)

    for d in range(1, sp):
        peer = lax.rem(me_sp + d, sp)
        when_owner(peer, lambda d=d: part_copy(d)[1].start())

    fetches["latent"].wait()

    def slot_of(d, c):
        return lax.rem(chip - d + chips, chips) * 2 + c

    row_copies = [
        remote(
            rows_v.at[me_tp], rows_v.at[me_tp], row_s.at[d - 1], row_r.at[d - 1],
            sp=me_sp, tp=lax.rem(chip + d, chips) * 2 + core,
        )
        for d in range(1, chips)
    ]
    relay_copies = [
        remote(
            rows_v.at[slot_of(d, core)], rows_v.at[slot_of(d, core)], relay_s.at[d], relay_r.at[d],
            sp=me_sp, tp=sibling,
        )
        for d in range(chips)
    ]
    relay_arrivals = [
        remote(
            rows_v.at[slot_of(d, 1 - core)], rows_v.at[slot_of(d, 1 - core)], relay_s.at[d], relay_r.at[d],
            sp=me_sp, tp=sibling,
        )
        for d in range(chips)
    ]
    row_arrivals = [
        remote(
            rows_v.at[slot_of(d, core)], rows_v.at[slot_of(d, core)], row_s.at[d - 1], row_r.at[d - 1],
            sp=me_sp, tp=lax.rem(chip + d, chips) * 2 + core,
        )
        for d in range(1, chips)
    ]
    for copy in row_copies:
        copy.start()
    relay_copies[0].start()

    my_slot = me_tp * plan.owners + me_sp
    vector_copies = [
        remote(
            vectors_v.at[my_slot], vectors_v.at[my_slot], vec_s.at[a * tp + b], vec_r.at[a * tp + b],
            sp=lax.rem(me_sp + a, sp), tp=lax.rem(me_tp + b, tp),
        )
        for a, b in everyone
    ]

    def own_columns():
        total = parts_v[me_sp]
        for d in range(1, sp):
            part_copy(d)[1].wait_recv()
            total = total + part_in_v[d - 1]
        vectors_v[my_slot] = total
        for copy in vector_copies:
            copy.start()

    when_owner(me_sp, own_columns)

    fetch("decay_up", 9, decay_up_hbm, wup_v.at[0])
    fetch("rate_up", 10, rate_up_hbm, wup_v.at[1])
    fetch("query", 11, query_hbm, wbig_v.at[2])
    fetch("branch", 12, branch_hbm, wbig_v.at[3])

    def inverse_of(x):
        x = x.astype(F32)
        mean = jnp.sum(x * x, axis=-1, keepdims=True) * (1.0 / depth)
        return jnp.broadcast_to(lax.rsqrt(mean + NORM_EPS), (16, 128))

    fetches["context"].wait()
    for at in range(0, plan.context_rows, 16):
        inverse_v[(plan.rows + at) // 16] = inverse_of(context_v[at : at + 16])

    def block_inverse(slot):
        for at in range(0, block, 16):
            inverse_v[(slot * block + at) // 16] = inverse_of(rows_v[slot, at : at + 16])

    block_inverse(me_tp)
    relay_arrivals[0].wait_recv()
    block_inverse(sibling)
    for d in range(1, chips):
        row_arrivals[d - 1].wait_recv()
        relay_copies[d].start()
        block_inverse(slot_of(d, core))
    for d in range(1, chips):
        relay_arrivals[d].wait_recv()
        block_inverse(slot_of(d, 1 - core))
    for p in range(packs):
        bias_v[p] = bias_ref[:, p * width : (p + 1) * width]

    for a, b in everyone:
        from_sp, from_tp = lax.rem(me_sp - a + sp, sp), lax.rem(me_tp - b + tp, tp)
        slot = from_tp * plan.owners + from_sp

        def take(a=a, b=b, slot=slot):
            remote(
                vectors_v.at[slot], vectors_v.at[slot], vec_s.at[a * tp + b], vec_r.at[a * tp + b],
                sp=me_sp, tp=me_tp,
            ).wait_recv()

        when_owner(from_sp, take)

    for j in range(tp * plan.owners):
        c = slice(j * plan.chunk, (j + 1) * plan.chunk)
        tile = vectors_v[j]
        mod_v[0:2, c] = norm_gain_ref[:, c] * (1.0 + tile[2:4])
        mod_v[2:4, c] = tile[0:2]
        gate_v[:, c] = tile[4:5]

    def modulate(read, group, which):
        inverse = inverse_v[group][:, 0:1]
        for at in range(0, depth, 512):
            c = slice(at, at + 512)
            x = read(c).astype(F32) * inverse * mod_v[which : which + 1, c] + mod_v[2 + which : 3 + which, c]
            normed_v[pl.ds(pl.multiple_of(group * 16, 16), 16), c] = x.astype(BF16)

    per = block // 16

    @pl.loop(0, plan.rows // 16)
    def _(g):
        slot, at = g // per, lax.rem(g, per) * 16
        modulate(lambda c: rows_v[slot, pl.ds(pl.multiple_of(at, 16), 16), c], g, 0)

    for at in range(0, plan.context_rows, 16):
        modulate(lambda c: context_v[at : at + 16, c], (plan.rows + at) // 16, 1)

    fetch("out", 13, out_hbm, wout_v)

    rank = decay_down_hbm.shape[1]
    fetches["decay_down"].wait()
    fetches["rate_down"].wait()
    low = jnp.dot(normed_v[...], wdown_v[...], preferred_element_type=F32)
    decay_low = jnp.tanh(low[:, :rank]).astype(BF16)
    rate_low = low[:, rank:].astype(BF16)

    def spread(found, at, target, kind):
        found = found.astype(BF16)
        for p in range(found.shape[1] // width):
            piece = found[:, p * width : (p + 1) * width]
            target[at // width + p] = piece[: plan.rows]
            if kind is not None:
                feature_out_v[at // width + p, kind] = piece[plan.rows :]

    for name, lhs, which, target, kind in (
        ("decay_up", decay_low, 0, decay_v, 2),
        ("rate_up", rate_low, 1, rate_v, 3),
    ):
        fetches[name].wait()
        for at in range(0, local, plan.tile):
            found = jnp.dot(lhs, wup_v[which, :, at : at + plan.tile], preferred_element_type=F32)
            spread(found, at, target, kind)

    def project(name, which, rows, target, kind):
        fetches[name].wait()
        for at in range(0, local, plan.tile):
            found = jnp.dot(
                normed_v[0:rows], wbig_v[which, :, at : at + plan.tile], preferred_element_type=F32
            )
            spread(found, at, target, kind)

    everything = plan.rows + plan.context_rows
    project("key", 0, everything, key_v, 0)
    project("value", 1, everything, value_v, 1)

    def pack_of(d):
        return (d * units) // 2

    def feature_copy(d):
        peer = lax.rem(me_sp + d, sp)
        return remote(
            feature_out_v.at[pack_of(peer)], feature_in_v.at[me_sp], feat_s.at[d - 1], feat_r.at[d - 1],
            sp=peer, tp=me_tp,
        )

    for d in range(1, sp):
        feature_copy(d).start()
    feature_in_v[me_sp] = feature_out_v[pack_of(me_sp)]

    project("query", 2, plan.rows, query_v, None)

    def maps_copy(d):
        peer = lax.rem(me_sp + d, sp)
        return remote(
            maps_out_v.at[pl.ds(peer * units, units)], maps_in_v.at[me_sp], map_s.at[d - 1], map_r.at[d - 1],
            sp=peer, tp=me_tp,
        )

    blocks = plan.rows // BLOCK
    group = min(2, packs)
    first = pack_of(me_sp)

    @pl.loop(0, packs // group)
    def _(s):
        at = [lax.rem(first + 1 + s * group + i, packs) for i in range(group)]
        items = []
        for p in at:
            k, erase, write, log_decay = chain_inputs(key_v[p], decay_v[p], rate_v[p], bias_v[p])
            items += solve_pack(k, value_v[p], erase, write, log_decay, query_v[p].astype(F32), (1, -1))
        found = solve_blocks(items, width)
        for i, p in enumerate(at):
            bases = [None] * blocks
            for way in (0, 1):
                mine = found[(i * 2 + way) * blocks : (i * 2 + way + 1) * blocks]
                carried = None
                for b in range(blocks) if way == 0 else reversed(range(blocks)):
                    transfer, constant, query, base = mine[b]
                    if carried is not None:
                        base = base + mmt(query, carried[1])
                        query = mmt(query, carried[0])
                        transfer, constant = (
                            mm(carried[0], transfer),
                            mm(carried[1], transfer) + constant,
                        )
                    carried = (transfer, constant)
                    reads_q_v[p, way, b * BLOCK : (b + 1) * BLOCK] = query.astype(BF16)
                    bases[b] = base if bases[b] is None else bases[b] + base
                maps_out_v[p * 2 + way, 0] = pack_heads(carried[0]).astype(BF16)
                maps_out_v[p * 2 + way, 1] = pack_heads(carried[1]).astype(BF16)
            for b in range(blocks):
                base_v[p, b * BLOCK : (b + 1) * BLOCK] = bases[b]
            if units == 2:
                d = 1 + s * group + i

                @pl.when(d < sp)
                def _():
                    maps_copy(d).start()

    if units == 1:
        for d in range(1, sp):
            maps_copy(d).start()
    maps_in_v[me_sp] = maps_out_v[pl.ds(me_sp * units, units)]

    for d in range(1, sp):
        source = lax.rem(me_sp - d + sp, sp)
        remote(
            feature_out_v.at[0], feature_in_v.at[source], feat_s.at[d - 1], feat_r.at[d - 1],
            sp=me_sp, tp=me_tp,
        ).wait_recv()
    keys, vals, decay_pre, rate_pre = (
        jnp.concatenate([feature_in_v[at, kind] for at in range(sp)], axis=0) for kind in range(4)
    )
    k, erase, write, log_decay = chain_inputs(keys, decay_pre, rate_pre, bias_v[first])
    count = plan.context_blocks
    if units == 2:
        signs, ways = (1, -1), (0, 1)
    else:
        ways = (lax.rem(me_sp, 2),)
        signs = (1 - 2 * ways[0],)
    found = solve_blocks(solve_pack(k, vals, erase, write, log_decay, None, signs), width)
    states = []
    for u in range(units):
        mine = found[u * count : (u + 1) * count]
        if units == 2:
            order = mine if u == 0 else mine[::-1]
            state = order[0][1]
            state = pack_heads(state)
            for transfer, constant, _, _ in order[1:]:
                state = advance(state, transfer, pack_heads(constant))
        else:
            for b, (transfer, constant, _, _) in enumerate(mine):
                transfer_v[b] = transfer.astype(BF16)
                constant_v[b] = pack_heads(constant)
            state = constant_v[jnp.where(ways[0] == 1, count - 1, 0)]
            for step in range(1, count):
                b = jnp.where(ways[0] == 1, count - 1 - step, step)
                state = advance(state, transfer_v[b], constant_v[b])
        states.append(state)

    project("branch", 3, plan.rows, branch_v, None)

    for d in range(1, sp):
        source = lax.rem(me_sp - d + sp, sp)
        remote(
            maps_out_v.at[pl.ds(0, units)], maps_in_v.at[source], map_s.at[d - 1], map_r.at[d - 1],
            sp=me_sp, tp=me_tp,
        ).wait_recv()

    def entry_copy(u, at):
        return remote(
            entry_out_v.at[at, u], entry_in_v.at[me_sp * units + u],
            ent_s.at[u, lax.rem(at - me_sp + sp, sp)], ent_r.at[u, lax.rem(at - me_sp + sp, sp)],
            sp=at, tp=me_tp,
        )

    for step in range(sp):
        for u in range(units):
            if units == 2:
                at = step if u == 0 else sp - 1 - step
            else:
                at = jnp.where(ways[0] == 1, sp - 1 - step, step)
            entry_out_v[at, u] = states[u].astype(BF16)

            @pl.when(at != me_sp)
            def _(u=u, at=at):
                entry_copy(u, at).start()

        if step < sp - 1:
            for u in range(units):
                if units == 2:
                    at = step if u == 0 else sp - 1 - step
                else:
                    at = jnp.where(ways[0] == 1, sp - 1 - step, step)
                states[u] = advance(
                    states[u], stack_heads(maps_in_v[at, u, 0]), maps_in_v[at, u, 1].astype(F32)
                )
    for u in range(units):
        entry_in_v[me_sp * units + u] = entry_out_v[me_sp, u]

    for d in range(1, sp):
        source = lax.rem(me_sp - d + sp, sp)
        for u in range(units):
            remote(
                entry_out_v.at[0, u], entry_in_v.at[source * units + u], ent_s.at[u, d], ent_r.at[u, d],
                sp=me_sp, tp=me_tp,
            ).wait_recv()

    ones = head_ones(width)
    for p in range(packs):
        c = slice(p * width, (p + 1) * width)
        reads = base_v[p]
        for way in (0, 1):
            reads = reads + mmt(reads_q_v[p, way], stack_heads(entry_in_v[2 * p + way]))
        away = reads - group_sum(reads, ones) * (1.0 / HEAD_DIM)
        variance = group_sum(away * away, ones) * (1.0 / HEAD_DIM)
        gates = branch_v[p].astype(F32)
        mixed_v[:, c] = (
            away * lax.rsqrt(variance + GROUP_EPS) * group_gain_ref[:, c] * (gates * jax.nn.sigmoid(gates))
        ).astype(BF16)

    fetches["out"].wait()

    def pair_copy(j):
        return remote(
            partial_v.at[j, 1 - core], pair_v.at[j], pair_s.at[j], pair_r.at[j], sp=me_sp, tp=sibling
        )

    def cross_copy(j, d):
        return remote(
            cross_out_v.at[j, d - 1], cross_in_v.at[j, d - 1], cross_s.at[j, d - 1], cross_r.at[j, d - 1],
            sp=me_sp, tp=lax.rem(chip + d, chips) * 2 + core,
        )

    for j in range(plan.out_tiles + 1):
        if j < plan.out_tiles:
            c = slice(j * plan.out_tile, (j + 1) * plan.out_tile)
            found = mm(mixed_v[...], wout_v[:, c]).astype(BF16)
            for t in range(tp):
                partial_v[j, t % 2, t // 2] = found[t * block : (t + 1) * block]
            pair_copy(j).start()
        if j > 0:
            i = j - 1
            pair_copy(i).wait_recv()
            for d in range(1, chips):
                to = lax.rem(chip + d, chips)
                cross_out_v[i, d - 1] = (
                    partial_v[i, core, to].astype(F32) + pair_v[i, to].astype(F32)
                ).astype(BF16)
                cross_copy(i, d).start()
    square = jnp.zeros((block, 1), F32)
    for j in range(plan.out_tiles):
        c = slice(j * plan.out_tile, (j + 1) * plan.out_tile)
        total = partial_v[j, core, chip].astype(F32) + pair_v[j, chip].astype(F32)
        for d in range(1, chips):
            cross_copy(j, d).wait_recv()
            total = total + cross_in_v[j, d - 1].astype(F32)
        total = total.astype(BF16).astype(F32)
        mixer_v[:, c] = total
        square = square + jnp.sum(total * total, axis=-1, keepdims=True)
    inverse = lax.rsqrt(square * (1.0 / depth) + NORM_EPS)
    for at in range(0, depth, 512):
        c = slice(at, at + 512)
        updated_ref[:, c] = (
            rows_v[me_tp, :, c].astype(F32) + gate_v[:, c] * (mixer_v[:, c] * inverse)
        ).astype(BF16)

    for d in range(1, sp):
        when_owner(lax.rem(me_sp + d, sp), lambda d=d: part_copy(d)[1].wait_send())
    for copy in row_copies + relay_copies:
        copy.wait_send()

    def vectors_left():
        for copy in vector_copies:
            copy.wait_send()

    when_owner(me_sp, vectors_left)
    for d in range(1, sp):
        feature_copy(d).wait_send()
        maps_copy(d).wait_send()
        for u in range(units):
            entry_copy(u, lax.rem(me_sp + d, sp)).wait_send()
    for j in range(plan.out_tiles):
        pair_copy(j).wait_send()
        for d in range(1, chips):
            cross_copy(j, d).wait_send()


def on_device(
    latent,
    context,
    condition,
    context_condition,
    shift_weight,
    scale_weight,
    gate_weight,
    norm_gain,
    decay_down,
    decay_up,
    rate_down,
    rate_up,
    head_bias,
    query_weight,
    key_weight,
    value_weight,
    branch_weight,
    group_gain,
    out_weight,
):
    sp, tp = lax.axis_size("sp"), lax.axis_size("tp")
    block, depth = latent.shape
    local = query_weight.shape[1]
    plan = Plan(sp, tp, block, context.shape[0], depth, local)
    width, packs, units, chips = plan.width, plan.packs, plan.units, plan.chips
    rows, crows, tiles = plan.rows, plan.context_rows, plan.out_tiles
    rank = decay_down.shape[1]
    vmem = pl.BlockSpec(memory_space=pltpu.VMEM)
    hbm = pl.BlockSpec(memory_space=pltpu.HBM)
    scratch = [
        ((tp, block, depth), BF16),
        ((crows, depth), BF16),
        ((3, *shift_weight.shape), BF16),
        ((depth, 2 * rank), BF16),
        ((2, rank, local), BF16),
        ((4, depth, local), BF16),
        ((local, depth), BF16),
        ((plan.owners, 8, plan.chunk), F32),
        ((sp - 1, 8, plan.chunk), F32),
        ((tp * plan.owners, 8, plan.chunk), F32),
        ((8, depth), F32),
        ((1, depth), F32),
        (((rows + crows) // 16, 16, 128), F32),
        ((rows + crows, depth), BF16),
        ((packs, rows, width), BF16),
        ((packs, rows, width), BF16),
        ((packs, rows, width), BF16),
        ((packs, rows, width), BF16),
        ((packs, rows, width), BF16),
        ((packs, rows, width), BF16),
        ((packs, 2, width), F32),
        ((packs, 4, crows, width), BF16),
        ((sp, 4, crows, width), BF16),
        ((2 * packs, 2, HEAD_DIM, width), BF16),
        ((sp, units, 2, HEAD_DIM, width), BF16),
        ((packs, 2, rows, width), BF16),
        ((packs, rows, width), F32),
        ((plan.context_blocks, width, width), BF16),
        ((plan.context_blocks, HEAD_DIM, width), F32),
        ((sp, units, HEAD_DIM, width), BF16),
        ((2 * packs, HEAD_DIM, width), BF16),
        ((rows, local), BF16),
        ((tiles, 2, chips, block, plan.out_tile), BF16),
        ((tiles, chips, block, plan.out_tile), BF16),
        ((tiles, chips - 1, block, plan.out_tile), BF16),
        ((tiles, chips - 1, block, plan.out_tile), BF16),
        ((block, depth), F32),
    ]
    semaphores = [
        (14,),
        (chips - 1,), (chips - 1,), (chips,), (chips,), (sp - 1,), (sp - 1,), (sp * tp,), (sp * tp,),
        (sp - 1,), (sp - 1,), (sp - 1,), (sp - 1,), (units, sp), (units, sp),
        (tiles,), (tiles,), (tiles, chips - 1), (tiles, chips - 1),
    ]
    return pl.pallas_call(
        functools.partial(layer_kernel, plan),
        in_specs=[hbm, hbm, vmem, vmem, hbm, hbm, hbm, vmem, hbm, hbm, hbm, hbm, vmem, hbm, hbm, hbm, hbm, vmem, hbm],
        out_specs=vmem,
        out_shape=jax.ShapeDtypeStruct(latent.shape, BF16),
        scratch_shapes=[pltpu.VMEM(shape, kind) for shape, kind in scratch]
        + [pltpu.SemaphoreType.DMA(shape) for shape in semaphores],
        compiler_params=pltpu.CompilerParams(
            collective_id=0, has_side_effects=True, vmem_limit_bytes=67043328
        ),
        name="layer",
    )(
        latent, context, condition.reshape(1, -1), context_condition.reshape(1, -1),
        shift_weight, scale_weight, gate_weight, norm_gain.reshape(1, -1),
        decay_down, decay_up, rate_down, rate_up, head_bias,
        query_weight, key_weight, value_weight, branch_weight, group_gain.reshape(1, -1), out_weight,
    )


def solution(mesh):
    placed = (
        P(("sp", "tp"), None),
        P("sp", None),
        P("sp"),
        P("sp"),
        P("sp", "tp"),
        P("sp", "tp"),
        P("sp", "tp"),
        P(),
        P(),
        P(None, "tp"),
        P(),
        P(None, "tp"),
        P(None, "tp"),
        P(None, "tp"),
        P(None, "tp"),
        P(None, "tp"),
        P(None, "tp"),
        P("tp"),
        P("tp", None),
    )
    return jax.shard_map(
        on_device, mesh=mesh, in_specs=placed, out_specs=P(("sp", "tp"), None), check_vma=False
    )
```

time: 127 us -> 65 us (0.51)
  matrix products: 29.1 us -> 0 us
  waiting for transfers between devices: 18.8 us -> 0 us
  starting transfers between devices: 15.4 us -> 0 us
  Pallas kernels: 49 us -> 63.1 us
  other arithmetic: 9.46 us -> 0 us
  local copies, waits for them, and re-layouts: 3.94 us -> 1.67 us
    dot_general x8 -> x0, matrix products: 29.1 us -> none  [the longest x6 23.2 us: project(): return jnp.dot(rows, weight, preferred_element_type=F32).astype(BF16)]
    pallas_call x5 -> x1, Pallas kernels: 49 us -> 63.1 us  [on_device(): pl.pallas_call(functools.partial(layer_kernel, plan), in_specs=[hbm, hbm,...]
    all_to_all x3 -> x0, starting transfers between devices: 13.1 us -> none  [the longest x1 5.95 us: on_device(): lax.all_to_all(maps.reshape(devices, own, 2, HEAD_DIM, width), 'sp', spli...]
    all_to_all x3 -> x0, waiting for transfers between devices: 12.3 us -> none  [the longest x1 8.54 us: on_device(): lax.all_to_all(maps.reshape(devices, own, 2, HEAD_DIM, width), 'sp', spli...]
    ppermute x4 -> x0, waiting for transfers between devices: 6.49 us -> none  [the longest x2 6.02 us: summed_rows(): lax.ppermute(block, 'tp', [(at, (at + 2 * d) % tp) for at in range(tp)])]
    reduce_sum x3 -> x0, other arithmetic: 2.9 us -> none  [the longest x2 2.73 us: modulated(): jnp.mean(values * values, axis=-1, keepdims=True) + NORM_EPS]
    convert_element_type x5 -> x0, other arithmetic: 2.76 us -> none  [the longest x2 1.84 us: modulated(): return (values * inverse * gain * (1.0 + scale) + shift).astype(BF16)]
    ppermute x4 -> x0, starting transfers between devices: 2.31 us -> none  [the longest x2 1.69 us: summed_rows(): lax.ppermute(block, 'tp', [(at, (at + 2 * d) % tp) for at in range(tp)])]
  transfers between devices with their start and end apart: 7 -> 0, of which waited for: 5 -> 0; matrix products, arithmetic and copies ran while one was open for 12% -> 0% of each run, Pallas kernels for 15% -> 0%
where the time goes in v1:
time: 65 us; the launch traced here: 64.8 us
  Pallas kernels  63.1 us (97%)
  local copies, waits for them, and re-layouts  1.67 us (3%)
    pallas_call x1, Pallas kernels, on_device(): pl.pallas_call(functools.partial(layer_kernel, plan), in_specs=[hbm, hbm,...  63.1 us
    unnamed x1, local copies, waits for them, and re-layouts  1.67 us

profile of v1, /device:TPU:0, one launch (start us, length us, event | category | flops | bytes accessed | tf_op | source)
XLA Modules:
  0.0 64.8 jit_solution(3047840371195042138)
XLA Ops:
  0.0 63.1 %layer.1 = bf16[32,4096]{1,0:T(8,128)(2,1)} custom-call(bf16[32,4096]{1,0:T(8,128)(2,1)} %latent_hbm.1, bf16[32,4096]{1,0:T(8,128)(2,1)} %context_hbm.1, f32[1,512]{1,0:T(1,128)} %bitcast.6, f32[1,512]{1,0:T(1,128)} %bitcast.7, bf16[512,1024]{1,0:T(8,128)(2,1)} %shift_hbm.1, bf16[512,1024]{1,0:T(8,128)(2,1)} %scale_hbm.1, bf16[512,1024]{1,0:T(8,128)(2,1)} %gate_hbm.1, ...), custom_call_target="tpu_custom_call" | custom-call | tf_op jit(solution)/shard_map/layer/pallas_call | solution.py:750
  63.1 1.7 %copy.21 = bf16[32,4096]{1,0:T(8,128)(2,1)} copy(bf16[32,4096]{1,0:T(8,128)(2,1)} %layer.1) | data formatting | bytes 524288

commit v2 on v1

v2 whole, which is shorter than its diff:
```python
import functools
import math

import jax
import jax.numpy as jnp
from jax import lax
from jax.experimental import pallas as pl
from jax.experimental.pallas import tpu as pltpu
from jax.sharding import PartitionSpec as P

HEAD_DIM = 64
NORM_EPS = 1e-06
GROUP_EPS = 0.00064
DECAY_TOP = math.exp(-0.5)
BLOCK = 64
VMEM_BYTES = 67043328
F32, BF16 = jnp.float32, jnp.bfloat16


def dot_dims(a, b, left, right):
    return lax.dot_general(
        a.astype(BF16), b.astype(BF16), (((left,), (right,)), ((), ())), preferred_element_type=F32
    )


def mm(a, b):
    return dot_dims(a, b, 1, 0)


def mmt(a, b):
    return dot_dims(a, b, 1, 1)


def tmm(a, b):
    return dot_dims(a, b, 0, 0)


def parts_of(x, count):
    found = []
    for _ in range(count):
        part = x.astype(BF16)
        found.append(part)
        x = x - part.astype(F32)
    return found


def head_ones(width):
    row = lax.broadcasted_iota(jnp.int32, (width, width), 0) // HEAD_DIM
    col = lax.broadcasted_iota(jnp.int32, (width, width), 1) // HEAD_DIM
    return (row == col).astype(F32)


def group_sum(x, ones, count=3):
    return sum(mm(part, ones) for part in parts_of(x, count))


def stack_heads(x):
    x = x.astype(BF16)
    count = x.shape[1] // HEAD_DIM
    if count == 1:
        return x
    lane = lax.broadcasted_iota(jnp.int32, (1, x.shape[1]), 1) // HEAD_DIM
    return jnp.concatenate([x * (lane == h).astype(F32).astype(BF16) for h in range(count)], axis=0)


def pack_heads(x):
    return sum(x[at : at + HEAD_DIM] for at in range(0, x.shape[0], HEAD_DIM))


def chain_inputs(keys, decay_pre, rate_pre, head_bias):
    k = keys.astype(F32)
    log_decay = -DECAY_TOP * jax.nn.sigmoid(head_bias[0:1] + decay_pre.astype(F32))
    rate = jax.nn.sigmoid(head_bias[1:2] + rate_pre.astype(F32))
    unit = k * lax.rsqrt(group_sum(k * k, head_ones(k.shape[1]), 2) + 1.0)
    return k, -unit, unit * rate, log_decay


def block_sums(log_decay):
    size = log_decay.shape[0]
    row = lax.broadcasted_iota(jnp.int32, (size, size), 0)
    col = lax.broadcasted_iota(jnp.int32, (size, size), 1)
    mask = ((row >= col) & (row // BLOCK == col // BLOCK)).astype(F32)
    return sum(mm(mask, part) for part in parts_of(log_decay, 3))


def pack_items(k, v, erase, write, log_decay, signs):
    items, ahead = [], block_sums(log_decay)
    for sign in signs:
        for at in range(0, k.shape[0], BLOCK):
            r = slice(at, at + BLOCK)
            total = ahead[at + BLOCK - 1 : at + BLOCK]
            cum = ahead[r]
            if not isinstance(sign, int):
                cum = jnp.where(sign > 0, cum, total - cum + log_decay[r])
            elif sign < 0:
                cum = total - cum + log_decay[r]
            items.append((sign, k[r], v[r], erase[r], write[r], log_decay[r], cum, total))
    return items


def signed_masks(sign, width):
    row = lax.broadcasted_iota(jnp.int32, (BLOCK, width), 0)
    col = lax.broadcasted_iota(jnp.int32, (BLOCK, width), 1) % BLOCK
    return (row - col) * sign > 0, (row - col) * sign >= 0


def beside(left, right):
    return jnp.concatenate([stack_heads(left), stack_heads(right)], axis=1)


def above(left, right):
    return jnp.concatenate([stack_heads(left), stack_heads(right)], axis=0)


def solve_maps(items, width):
    row = lax.broadcasted_iota(jnp.int32, (BLOCK, width), 0)
    col = lax.broadcasted_iota(jnp.int32, (BLOCK, width), 1) % BLOCK
    ones = head_ones(width)
    square = lax.broadcasted_iota(jnp.int32, (width, width), 0)
    unit = (square == lax.broadcasted_iota(jnp.int32, (width, width), 1)).astype(F32)
    one = (row == col).astype(F32)
    near = (row // 2 == col // 2) & (row != col)
    work = []
    for sign, k, v, erase, write, log_decay, cum, total in items:
        strict, _ = signed_masks(sign, width)
        growth = jnp.exp(-cum)
        item = {"es": (erase * jnp.exp(cum - log_decay)).astype(BF16), "v": v.astype(BF16), "cum": cum}
        item["wg"], item["kg"] = (write * growth).astype(BF16), (k * growth).astype(BF16)
        both = mmt(item["es"], above(item["wg"], item["kg"]))
        item["coupling"] = jnp.where(strict, both[:, :width], 0.0)
        item["feed"] = jnp.where(strict, both[:, width:], 0.0)
        tail = jnp.exp(total - cum)
        item["wt"], item["kt"] = (write * tail).astype(BF16), (k * tail).astype(BF16)
        item["diagonal"] = unit * jnp.exp(total)
        work.append(item)
    for item in work:
        item["x"] = one + jnp.where(near, item["coupling"], 0.0)
        item["fed"] = mm(item["feed"], stack_heads(item["v"]))
    size = 2
    while size < BLOCK:
        level = (row // (2 * size) == col // (2 * size)) & (row // size != col // size)
        for item in work:
            item["y"] = mm(jnp.where(level, item["coupling"], 0.0), stack_heads(item["x"]))
        for item in work:
            item["x"] = item["x"] + mm(item["x"], stack_heads(item["y"]))
        size *= 2
    for item in work:
        both = mm(item["x"], beside(item["es"], item["fed"])).astype(BF16)
        item["both"] = both
        item["response"], item["offset"] = both[:, :width], both[:, width:]
    for item in work:
        moved = tmm(item["both"], item["wt"])
        item["transfer"] = moved[:width] * ones + item["diagonal"]
        item["constant"] = (moved[width:] + tmm(item["v"], item["kt"])) * ones
    return work


MESH = pl.DeviceIdType.MESH


def advance(state, transfer, constant):
    high, low = parts_of(state, 2)
    both = mm(jnp.concatenate([high, low], axis=0), transfer)
    return both[:HEAD_DIM] + both[HEAD_DIM:] + constant


class Plan:
    def __init__(self, sp, tp, rows, context_rows, depth, local):
        self.sp, self.tp, self.chips = sp, tp, tp // 2
        self.block, self.context_rows = rows, context_rows
        self.rows = rows * tp
        self.depth, self.local = depth, local
        heads = local // HEAD_DIM
        self.width = (2 if heads % sp == 0 else 1) * HEAD_DIM
        self.packs = local // self.width
        self.units = 2 * self.packs // sp
        assert self.units in (1, 2) and self.units * sp == 2 * self.packs
        self.half = sp // 2
        self.fold = self.packs // self.half
        assert self.half * 2 == sp and self.fold * self.half == self.packs
        self.group = min(4, self.packs)
        self.groups = self.packs // self.group
        self.pieces = 2 if rows % 32 == 0 else 1
        self.chunk = max(128, local // sp)
        self.owners = local // self.chunk
        self.tile = 512
        self.out_tile = local
        self.out_tiles = depth // self.out_tile
        self.context_blocks = context_rows * sp // BLOCK


def remote(source, target, sent, taken, **peer):
    return pltpu.make_async_remote_copy(
        src_ref=source,
        dst_ref=target,
        send_sem=sent,
        recv_sem=taken,
        device_id=peer,
        device_id_type=MESH,
    )


def layer_kernel(
    plan,
    latent_hbm, context_hbm, condition_ref, context_condition_ref,
    shift_hbm, scale_hbm, gate_hbm, norm_gain_ref,
    decay_down_hbm, decay_up_hbm, rate_down_hbm, rate_up_hbm, bias_ref,
    query_hbm, key_hbm, value_hbm, branch_hbm, group_gain_ref, out_hbm,
    updated_hbm,
    rows_v, context_v, wmod_v, wdown_v, wup_v, wbig_v,
    parts_v, part_in_v, vectors_v, gate_part_v, gate_in_v, gate_all_v, mod_v, inverse_v, normed_v,
    key_v, value_v, decay_v, rate_v, query_v, branch_v, bias_v,
    feature_out_v, feature_in_v, maps_out_v, maps_in_v, reads_q_v, base_v,
    saved_v, cum_v, first_v, transfer_v, constant_v,
    state_out_v, state_in_v, turn_out_v, turn_in_v, entry_out_v, entry_in_v, mixed_v,
    partial_v, pair_v, cross_out_v, cross_in_v, mixer_v,
    local_sem, row_s, row_r, relay_s, relay_r, part_s, part_r, vec_s, vec_r, gp_s, gp_r, gv_s, gv_r,
    feat_s, feat_r, map_s, map_r, st_s, st_r, turn_s, turn_r, ent_s, ent_r, pair_s, pair_r, cross_s, cross_r, store_sem,
):
    sp, tp, chips, width, packs, units = plan.sp, plan.tp, plan.chips, plan.width, plan.packs, plan.units
    depth, local, block = plan.depth, plan.local, plan.block
    half, fold, group, groups = plan.half, plan.fold, plan.group, plan.groups
    me_sp, me_tp = lax.axis_index("sp"), lax.axis_index("tp")
    chip, core = me_tp // 2, lax.rem(me_tp, 2)
    sibling = chip * 2 + 1 - core

    fetches = {}

    def fetch(name, at, source, target):
        copy = pltpu.make_async_copy(source, target, local_sem.at[at])
        copy.start()
        fetches[name] = copy

    fetch("shift", 0, shift_hbm, wmod_v.at[0])
    fetch("scale", 1, scale_hbm, wmod_v.at[1])
    fetch("gate", 2, gate_hbm, wmod_v.at[2])
    fetch("latent", 3, latent_hbm, rows_v.at[me_tp])
    fetch("context", 4, context_hbm, context_v)

    def settle(ref, semaphore):
        remote(ref, ref, semaphore, semaphore, sp=me_sp, tp=me_tp).wait_recv()

    peers = sorted(range(1, sp), key=lambda d: (abs(d - half), d))

    barrier = pltpu.get_barrier_semaphore()
    everyone = [(a, b) for a in range(sp) for b in range(tp) if (a, b) != (0, 0)]
    for a, b in everyone:
        pl.semaphore_signal(
            barrier,
            inc=1,
            device_id={"sp": lax.rem(me_sp + a, sp), "tp": lax.rem(me_tp + b, tp)},
            device_id_type=MESH,
        )

    line = lax.broadcasted_iota(jnp.int32, (8, condition_ref.shape[1]), 0)
    values = jnp.where(line == 0, condition_ref[...], jnp.where(line == 1, context_condition_ref[...], 0.0))
    conditions = (values * jax.nn.sigmoid(values)).astype(BF16)
    shares = []
    for at, name in enumerate(("shift", "scale", "gate")):
        fetches[name].wait()
        shares.append(mm(conditions, wmod_v[at])[0:2])
    fetch("decay_down", 5, decay_down_hbm, wdown_v.at[:, 0 : decay_down_hbm.shape[1]])
    fetch("rate_down", 5, rate_down_hbm, wdown_v.at[:, decay_down_hbm.shape[1] :])
    fetch("key", 7, key_hbm, wbig_v.at[0])
    fetch("value", 8, value_hbm, wbig_v.at[1])
    for j in range(plan.owners):
        c = slice(j * plan.chunk, (j + 1) * plan.chunk)
        parts_v[j, 0:2] = shares[0][:, c]
        parts_v[j, 2:4] = shares[1][:, c]
        gate_part_v[j] = shares[2][0:1, c]

    pl.semaphore_wait(barrier, len(everyone))

    def part_copy(d):
        peer = lax.rem(me_sp + d, sp)
        return peer, remote(
            parts_v.at[peer], part_in_v.at[d - 1], part_s.at[0], part_r.at[0], sp=peer, tp=me_tp
        )

    def gate_copy(d):
        peer = lax.rem(me_sp + d, sp)
        return remote(
            gate_part_v.at[peer], gate_in_v.at[d - 1], gp_s.at[0], gp_r.at[0], sp=peer, tp=me_tp
        )

    def when_owner(at, body):
        if plan.owners == sp:
            body()
        else:
            pl.when(at < plan.owners)(body)

    for d in range(1, sp):
        peer = lax.rem(me_sp + d, sp)
        when_owner(peer, lambda d=d: part_copy(d)[1].start())

    fetches["latent"].wait()

    def slot_of(d, c):
        return lax.rem(chip - d + chips, chips) * 2 + c

    piece = block // plan.pieces

    def row_copy(d, i, slot):
        part = rows_v.at[slot, pl.ds(i * piece, piece)]
        return remote(
            part, part, row_s.at[0], row_r.at[d - 1, i],
            sp=me_sp, tp=lax.rem(chip + d, chips) * 2 + core,
        )

    def relay_copy(d, i, c):
        part = rows_v.at[slot_of(d, c), pl.ds(i * piece, piece)]
        return remote(part, part, relay_s.at[0], relay_r.at[d], sp=me_sp, tp=sibling)

    row_copies = [row_copy(d, i, me_tp) for i in range(plan.pieces) for d in range(1, chips)]
    relay_copies = [relay_copy(d, i, core) for d in range(chips) for i in range(plan.pieces)]
    for copy in row_copies:
        copy.start()
    for i in range(plan.pieces):
        relay_copies[i].start()
    for d in range(1, sp):
        when_owner(lax.rem(me_sp + d, sp), lambda d=d: gate_copy(d).start())

    my_slot = me_tp * plan.owners + me_sp
    vector_copies = [
        remote(
            vectors_v.at[my_slot], vectors_v.at[my_slot], vec_s.at[0], vec_r.at[0],
            sp=lax.rem(me_sp + a, sp), tp=lax.rem(me_tp + b, tp),
        )
        for a, b in everyone
    ]

    def own_columns():
        total = parts_v[me_sp]
        settle(part_in_v, part_r.at[0])
        for d in range(1, sp):
            total = total + part_in_v[d - 1]
        vectors_v[my_slot] = total
        for copy in vector_copies:
            copy.start()

    when_owner(me_sp, own_columns)

    fetch("decay_up", 9, decay_up_hbm, wup_v.at[0])
    fetch("rate_up", 9, rate_up_hbm, wup_v.at[1])
    fetch("query", 11, query_hbm, wbig_v.at[2])
    fetch("branch", 12, branch_hbm, wbig_v.at[3])

    def inverse_of(x):
        x = x.astype(F32)
        mean = jnp.sum(x * x, axis=-1, keepdims=True) * (1.0 / depth)
        return jnp.broadcast_to(lax.rsqrt(mean + NORM_EPS), (16, 128))

    fetches["context"].wait()
    for at in range(0, plan.context_rows, 16):
        inverse_v[(plan.rows + at) // 16] = inverse_of(context_v[at : at + 16])

    def block_inverse(slot):
        for at in range(0, block, 16):
            inverse_v[(slot * block + at) // 16] = inverse_of(rows_v[slot, at : at + 16])

    for p in range(packs):
        bias_v[p] = bias_ref[:, p * width : (p + 1) * width]
    block_inverse(me_tp)
    settle(rows_v.at[sibling], relay_r.at[0])
    block_inverse(sibling)
    for i in range(plan.pieces):
        for d in range(1, chips):
            row_copy(d, i, slot_of(d, core)).wait_recv()
            relay_copies[d * plan.pieces + i].start()
    for d in range(1, chips):
        block_inverse(slot_of(d, core))
    for d in range(1, chips):
        settle(rows_v.at[slot_of(d, 1 - core)], relay_r.at[d])
        block_inverse(slot_of(d, 1 - core))

    def all_but_mine(ref, count, semaphore):
        if plan.owners == sp:
            settle(ref.at[pl.ds(0, count - 1)], semaphore)
        else:
            pl.when(me_sp < plan.owners)(lambda: settle(ref.at[pl.ds(0, count - 1)], semaphore))
            pl.when(me_sp >= plan.owners)(lambda: settle(ref.at[pl.ds(0, count)], semaphore))

    all_but_mine(vectors_v, tp * plan.owners, vec_r.at[0])

    for j in range(tp * plan.owners):
        c = slice(j * plan.chunk, (j + 1) * plan.chunk)
        tile = vectors_v[j]
        mod_v[0:2, c] = norm_gain_ref[:, c] * (1.0 + tile[2:4])
        mod_v[2:4, c] = tile[0:2]

    def modulate(read, group, which):
        inverse = inverse_v[group][:, 0:1]
        for at in range(0, depth, 512):
            c = slice(at, at + 512)
            x = read(c).astype(F32) * inverse * mod_v[which : which + 1, c] + mod_v[2 + which : 3 + which, c]
            normed_v[pl.ds(pl.multiple_of(group * 16, 16), 16), c] = x.astype(BF16)

    per = block // 16

    @pl.loop(0, plan.rows // 16)
    def _(g):
        slot, at = g // per, lax.rem(g, per) * 16
        modulate(lambda c: rows_v[slot, pl.ds(pl.multiple_of(at, 16), 16), c], g, 0)

    for at in range(0, plan.context_rows, 16):
        modulate(lambda c: context_v[at : at + 16, c], (plan.rows + at) // 16, 1)

    rank = decay_down_hbm.shape[1]
    settle(wdown_v, local_sem.at[5])
    settle(wup_v, local_sem.at[9])
    low = sum(
        jnp.dot(normed_v[:, c], wdown_v[c], preferred_element_type=F32)
        for c in (slice(0, depth // 2), slice(depth // 2, depth))
    )
    decay_low = jnp.tanh(low[:, :rank]).astype(BF16)
    rate_low = low[:, rank:].astype(BF16)

    gate_copies = [
        remote(
            gate_all_v.at[my_slot], gate_all_v.at[my_slot], gv_s.at[0], gv_r.at[0],
            sp=lax.rem(me_sp + a, sp), tp=lax.rem(me_tp + b, tp),
        )
        for a, b in everyone
    ]

    def own_gate():
        total = gate_part_v[me_sp]
        settle(gate_in_v, gp_r.at[0])
        for d in range(1, sp):
            total = total + gate_in_v[d - 1]
        gate_all_v[my_slot] = total
        for copy in gate_copies:
            copy.start()

    def spread(found, at, target, kind):
        found = found.astype(BF16)
        for p in range(found.shape[1] // width):
            piece = found[:, p * width : (p + 1) * width]
            target[at // width + p] = piece[: plan.rows]
            if kind is not None:
                feature_out_v[at // width + p, kind] = piece[plan.rows :]

    for name, lhs, which, target, kind in (
        ("decay_up", decay_low, 0, decay_v, 2),
        ("rate_up", rate_low, 1, rate_v, 3),
    ):
        for at in range(0, local, plan.tile):
            found = jnp.dot(lhs, wup_v[which, :, at : at + plan.tile], preferred_element_type=F32)
            spread(found, at, target, kind)

    def project(name, which, rows, target, kind):
        fetches[name].wait()
        for at in range(0, local, plan.tile):
            found = jnp.dot(
                normed_v[0:rows], wbig_v[which, :, at : at + plan.tile], preferred_element_type=F32
            )
            spread(found, at, target, kind)

    def pack_of(d):
        return (d * units) // 2

    def feature_part(at, i):
        return at.at[(pl.ds(2, 2), pl.ds(0, 1), pl.ds(1, 1))[i]]

    def feature_copy(d, i):
        peer = lax.rem(me_sp + d, sp)
        return remote(
            feature_part(feature_out_v.at[pack_of(peer)], i), feature_part(feature_in_v.at[me_sp], i),
            feat_s.at[0], feat_r.at[0], sp=peer, tp=me_tp,
        )

    everything = plan.rows + plan.context_rows
    for d in peers:
        feature_copy(d, 0).start()
    project("key", 0, everything, key_v, 0)
    for d in peers:
        feature_copy(d, 1).start()
    for j in range(plan.out_tiles):
        fetch("out", 6, out_hbm.at[:, j * local : (j + 1) * local], wbig_v.at[0, j * local : (j + 1) * local])
    project("value", 1, everything, value_v, 1)
    for d in peers:
        feature_copy(d, 2).start()
    feature_in_v[me_sp] = feature_out_v[pack_of(me_sp)]
    when_owner(me_sp, own_gate)

    side, index = me_sp // half, lax.rem(me_sp, half)
    blocks = plan.rows // BLOCK

    def map_copy(p):
        owner, slot = p // fold, lax.rem(p, fold)
        d = lax.rem(owner - index + half, half)
        return d, remote(
            maps_out_v.at[p], maps_in_v.at[index, slot], map_s.at[0], map_r.at[0],
            sp=side * half + owner, tp=me_tp,
        )

    def latent_maps(s):
        at = [lax.rem((index + 1) * fold + s * group + i, packs) for i in range(group)]
        items = []
        for p in at:
            k, erase, write, log_decay = chain_inputs(key_v[p], decay_v[p], rate_v[p], bias_v[p])
            items += pack_items(k, value_v[p], erase, write, log_decay, (1, -1))
        found = solve_maps(items, width)
        for i, p in enumerate(at):
            for way in (0, 1):
                mine = found[(i * 2 + way) * blocks : (i * 2 + way + 1) * blocks]
                carried = None
                for b in range(blocks) if way == 0 else reversed(range(blocks)):
                    item = mine[b]
                    transfer, constant = item["transfer"], item["constant"]
                    if carried is not None:
                        first_v[p, way, b, :width] = carried[0].astype(BF16)
                        first_v[p, way, b, width:] = carried[1].astype(BF16)
                        both = mm(jnp.concatenate(carried, axis=0), transfer)
                        transfer, constant = both[:width], both[width:] + constant
                    carried = (transfer, constant)
                    for kind, name in enumerate(("wg", "kg", "response", "offset")):
                        saved_v[p, way, b, kind] = item[name]
                    cum_v[p, way, b] = item["cum"]
                maps_out_v[p, way, 0] = pack_heads(carried[0]).astype(BF16)
                maps_out_v[p, way, 1] = pack_heads(carried[1]).astype(BF16)
            d, copy = map_copy(p)

            @pl.when(d != 0)
            def _(copy=copy):
                copy.start()

    pl.loop(0, groups)(latent_maps)
    for i in range(fold):
        maps_in_v[index, i] = maps_out_v[index * fold + i]

    settle(feature_in_v.at[pl.ds(0, sp - 1)], feat_r.at[0])
    keys, vals, decay_pre, rate_pre = (
        jnp.concatenate([feature_in_v[at, kind] for at in range(sp)], axis=0) for kind in range(4)
    )
    held = pack_of(me_sp)
    k, erase, write, log_decay = chain_inputs(keys, decay_pre, rate_pre, bias_v[held])
    count = plan.context_blocks
    if units == 2:
        ways = (0, 1)
    else:
        ways = (lax.rem(me_sp, 2),)
    found = solve_maps(pack_items(k, vals, erase, write, log_decay, [1 - 2 * way for way in ways]), width)

    def state_copy(u):
        target = ways[u] * half + held // fold
        slot = lax.rem(held, fold)
        return target, slot, remote(
            state_out_v.at[u], state_in_v.at[slot], st_s.at[u], st_r.at[slot], sp=target, tp=me_tp
        )

    for u in range(units):
        mine = found[u * count : (u + 1) * count]
        if units == 2:
            order = mine if u == 0 else mine[::-1]
            state = pack_heads(order[0]["constant"])
            for item in order[1:]:
                state = advance(state, item["transfer"], pack_heads(item["constant"]))
        else:
            for b, item in enumerate(mine):
                transfer_v[b] = item["transfer"].astype(BF16)
                constant_v[b] = pack_heads(item["constant"])
            state = constant_v[jnp.where(ways[0] == 1, count - 1, 0)]
            for step in range(1, count):
                b = jnp.where(ways[0] == 1, count - 1 - step, step)
                state = advance(state, transfer_v[b], constant_v[b])
        state_out_v[u] = state.astype(BF16)
        target, slot, copy = state_copy(u)

        @pl.when(target != me_sp)
        def _(copy=copy):
            copy.start()

        @pl.when(target == me_sp)
        def _(u=u, slot=slot):
            state_in_v[slot] = state_out_v[u]

    project("query", 2, plan.rows, query_v, None)

    def latent_queries(s):
        jobs = []
        for i in range(group):
            p = s * group + i
            for way in (0, 1):
                _, inclusive = signed_masks(1 - 2 * way, width)
                for b in range(blocks):
                    q = query_v[p, b * BLOCK : (b + 1) * BLOCK].astype(F32) * jnp.exp(cum_v[p, way, b])
                    jobs.append({"p": p, "way": way, "b": b, "q": q, "mask": inclusive})
        for job in jobs:
            p, way, b = job["p"], job["way"], job["b"]
            both = mmt(job["q"], above(saved_v[p, way, b, 0], saved_v[p, way, b, 1]))
            job["aw"] = jnp.where(job["mask"], both[:, :width], 0.0)
            job["ak"] = jnp.where(job["mask"], both[:, width:], 0.0)
        for job in jobs:
            p, way, b = job["p"], job["way"], job["b"]
            both = mm(job["aw"], beside(saved_v[p, way, b, 2], saved_v[p, way, b, 3]))
            job["query"] = job["q"] + both[:, :width]
            fed = mm(job["ak"], stack_heads(value_v[p, b * BLOCK : (b + 1) * BLOCK]))
            job["base"] = both[:, width:] + fed
        for job in jobs:
            p, way, b = job["p"], job["way"], job["b"]
            if b != (0 if way == 0 else blocks - 1):
                both = mmt(job["query"], first_v[p, way, b])
                job["query"] = both[:, :width]
                job["base"] = job["base"] + both[:, width:]
            reads_q_v[p, way, b * BLOCK : (b + 1) * BLOCK] = job["query"].astype(BF16)
        for i in range(group):
            mine = jobs[i * 2 * blocks : (i + 1) * 2 * blocks]
            for b in range(blocks):
                base_v[s * group + i, b * BLOCK : (b + 1) * BLOCK] = mine[b]["base"] + mine[blocks + b]["base"]

    def entry_copy(stage, way, at):
        return remote(
            entry_out_v.at[stage, at], entry_in_v.at[way, pl.ds(index * fold, fold)],
            ent_s.at[stage], ent_r.at[stage], sp=side * half + at, tp=me_tp,
        )

    def fold_maps(stage, way, start):
        states = [start[i].astype(F32) for i in range(fold)]
        for step in range(half):
            at = jnp.where(way == 0, step, half - 1 - step)
            for i in range(fold):
                entry_out_v[stage, at, i] = states[i].astype(BF16)

            @pl.when(at != index)
            def _(at=at):
                entry_copy(stage, way, at).start()

            if stage == 0 or step < half - 1:
                for i in range(fold):
                    states[i] = advance(
                        states[i], stack_heads(maps_in_v[at, i, way, 0]), maps_in_v[at, i, way, 1].astype(F32)
                    )
        for i in range(fold):
            entry_in_v[way, index * fold + i] = entry_out_v[stage, index, i]
        return states

    def entries_arrived(stage, way):
        settle(entry_in_v.at[way, pl.ds(0, (half - 1) * fold)], ent_r.at[stage])

    pl.loop(0, groups)(latent_queries)
    settle(maps_in_v.at[pl.ds(0, half - 1)], map_r.at[0])
    for i in range(fold):
        p = index * fold + i

        @pl.when((2 * p + side) // units != me_sp)
        def _(i=i):
            remote(
                state_out_v.at[0], state_in_v.at[i], st_s.at[0], st_r.at[i], sp=me_sp, tp=me_tp
            ).wait_recv()

    states = fold_maps(0, side, state_in_v)
    for i in range(fold):
        turn_out_v[i] = states[i].astype(BF16)
    turn = remote(
        turn_out_v, turn_in_v, turn_s.at[0], turn_r.at[0], sp=(1 - side) * half + index, tp=me_tp
    )
    turn.start()

    project("branch", 3, plan.rows, branch_v, None)
    turn.wait_recv()
    fold_maps(1, 1 - side, turn_in_v)

    entries_arrived(0, side)
    for p in range(packs):
        base_v[p] = base_v[p] + mmt(reads_q_v[p, side], stack_heads(entry_in_v[side, p]))
    entries_arrived(1, 1 - side)

    ones = head_ones(width)
    pair_rows = 2 * block

    def mixed_rows(e):
        at = pl.multiple_of(lax.rem(chip + e, chips) * pair_rows, pair_rows)
        r = pl.ds(at, pair_rows)
        found = [
            base_v[p, r] + mmt(reads_q_v[p, 1 - side, r], stack_heads(entry_in_v[1 - side, p]))
            for p in range(packs)
        ]
        away = [x - group_sum(x, ones, 2) * (1.0 / HEAD_DIM) for x in found]
        variance = [group_sum(x * x, ones, 2) * (1.0 / HEAD_DIM) for x in away]
        for p in range(packs):
            c = slice(p * width, (p + 1) * width)
            gates = branch_v[p, r].astype(F32)
            mixed_v[:, c] = (
                away[p] * lax.rsqrt(variance[p] + GROUP_EPS)
                * group_gain_ref[:, c] * (gates * jax.nn.sigmoid(gates))
            ).astype(BF16)

    def pair_copy(e, j):
        return remote(
            partial_v.at[e, j, 1 - core], pair_v.at[e, j], pair_s.at[0], pair_r.at[(e - 1) * plan.out_tiles + j if e else (chips - 1) * plan.out_tiles],
            sp=me_sp, tp=sibling,
        )

    def cross_copy(e, j):
        return remote(
            cross_out_v.at[e - 1, j], cross_in_v.at[e - 1, j], cross_s.at[0], cross_r.at[e - 1, j],
            sp=me_sp, tp=lax.rem(chip + e, chips) * 2 + core,
        )

    def out_copy(j):
        return pltpu.make_async_copy(
            mixer_v.at[:, j * local : (j + 1) * local], updated_hbm.at[:, j * local : (j + 1) * local], store_sem.at[0]
        )

    settle(wbig_v.at[0], local_sem.at[6])
    for e in [*range(1, chips), 0]:
        mixed_rows(e)
        for j in range(plan.out_tiles):
            found = mm(mixed_v[...], wbig_v[0, j * local : (j + 1) * local]).astype(BF16)
            for i in range(2):
                partial_v[e, j, i] = found[i * block : (i + 1) * block]
            pair_copy(e, j).start()
        if e > 0:
            for j in range(plan.out_tiles):
                pair_copy(e, j).wait_recv()
                cross_out_v[e - 1, j] = (
                    partial_v[e, j, core].astype(F32) + pair_v[e, j].astype(F32)
                ).astype(BF16)
                cross_copy(e, j).start()
    all_but_mine(gate_all_v, tp * plan.owners, gv_r.at[0])
    settle(pair_v.at[0], pair_r.at[(chips - 1) * plan.out_tiles])
    square = jnp.zeros((block, 1), F32)
    totals = []
    for j in range(plan.out_tiles):
        total = partial_v[0, j, core].astype(F32) + pair_v[0, j].astype(F32)
        for e in range(1, chips):
            cross_copy(e, j).wait_recv()
            total = total + cross_in_v[e - 1, j].astype(F32)
        total = total.astype(BF16)
        mixer_v[:, j * local : (j + 1) * local] = total
        total = total.astype(F32)
        square = square + jnp.sum(total * total, axis=-1, keepdims=True)
    inverse = lax.rsqrt(square * (1.0 / depth) + NORM_EPS)
    per_tile = local // plan.chunk
    for j in range(plan.out_tiles):
        for i in range(j * per_tile, (j + 1) * per_tile):
            c = slice(i * plan.chunk, (i + 1) * plan.chunk)
            mixer_v[:, c] = (
                rows_v[me_tp, :, c].astype(F32) + gate_all_v[i] * (mixer_v[:, c].astype(F32) * inverse)
            ).astype(BF16)
        out_copy(j).start()

    all_but_mine(parts_v, plan.owners, part_s.at[0])
    all_but_mine(gate_part_v, plan.owners, gp_s.at[0])
    settle(rows_v.at[pl.ds(0, chips - 1)], row_s.at[0])
    settle(rows_v.at[pl.ds(0, chips)], relay_s.at[0])

    def vectors_left():
        left = len(everyone)
        for ref, semaphore in ((vectors_v, vec_s.at[0]), (gate_all_v, gv_s.at[0])):
            whole, rest = left // ref.shape[0], left % ref.shape[0]
            for _ in range(whole):
                settle(ref, semaphore)
            if rest:
                settle(ref.at[pl.ds(0, rest)], semaphore)

    when_owner(me_sp, vectors_left)
    settle(feature_in_v.at[pl.ds(0, sp - 1)], feat_s.at[0])
    settle(maps_in_v.at[pl.ds(0, half - 1)], map_s.at[0])
    for stage in (0, 1):
        settle(entry_in_v.at[0, pl.ds(0, (half - 1) * fold)], ent_s.at[stage])
    for u in range(units):
        target, _, copy = state_copy(u)

        @pl.when(target != me_sp)
        def _(copy=copy):
            copy.wait_send()

    turn.wait_send()
    settle(pair_v, pair_s.at[0])
    settle(cross_out_v, cross_s.at[0])
    settle(mixer_v, store_sem.at[0])


def on_device(
    latent,
    context,
    condition,
    context_condition,
    shift_weight,
    scale_weight,
    gate_weight,
    norm_gain,
    decay_down,
    decay_up,
    rate_down,
    rate_up,
    head_bias,
    query_weight,
    key_weight,
    value_weight,
    branch_weight,
    group_gain,
    out_weight,
):
    sp, tp = lax.axis_size("sp"), lax.axis_size("tp")
    block, depth = latent.shape
    local = query_weight.shape[1]
    plan = Plan(sp, tp, block, context.shape[0], depth, local)
    width, packs, units, chips = plan.width, plan.packs, plan.units, plan.chips
    rows, crows, tiles = plan.rows, plan.context_rows, plan.out_tiles
    half, fold, blocks = plan.half, plan.fold, rows // BLOCK
    rank = decay_down.shape[1]
    vmem = pl.BlockSpec(memory_space=pltpu.VMEM)
    hbm = pl.BlockSpec(memory_space=pltpu.HBM)
    scratch = [
        ((tp, block, depth), BF16),
        ((crows, depth), BF16),
        ((3, *shift_weight.shape), BF16),
        ((depth, 2 * rank), BF16),
        ((2, rank, local), BF16),
        ((4, depth, local), BF16),
        ((plan.owners, 4, plan.chunk), F32),
        ((sp - 1, 4, plan.chunk), F32),
        ((tp * plan.owners, 4, plan.chunk), F32),
        ((plan.owners, 1, plan.chunk), F32),
        ((sp - 1, 1, plan.chunk), F32),
        ((tp * plan.owners, 1, plan.chunk), F32),
        ((8, depth), F32),
        (((rows + crows) // 16, 16, 128), F32),
        ((rows + crows, depth), BF16),
        ((packs, rows, width), BF16),
        ((packs, rows, width), BF16),
        ((packs, rows, width), BF16),
        ((packs, rows, width), BF16),
        ((packs, rows, width), BF16),
        ((packs, rows, width), BF16),
        ((packs, 2, width), F32),
        ((packs, 4, crows, width), BF16),
        ((sp, 4, crows, width), BF16),
        ((packs, 2, 2, HEAD_DIM, width), BF16),
        ((half, fold, 2, 2, HEAD_DIM, width), BF16),
        ((packs, 2, rows, width), BF16),
        ((packs, rows, width), F32),
        ((packs, 2, blocks, 4, BLOCK, width), BF16),
        ((packs, 2, blocks, BLOCK, width), F32),
        ((packs, 2, blocks, 2 * width, width), BF16),
        ((plan.context_blocks, width, width), BF16),
        ((plan.context_blocks, HEAD_DIM, width), F32),
        ((units, HEAD_DIM, width), BF16),
        ((fold, HEAD_DIM, width), BF16),
        ((fold, HEAD_DIM, width), BF16),
        ((fold, HEAD_DIM, width), BF16),
        ((2, half, fold, HEAD_DIM, width), BF16),
        ((2, packs, HEAD_DIM, width), BF16),
        ((2 * block, local), BF16),
        ((chips, tiles, 2, block, plan.out_tile), BF16),
        ((chips, tiles, block, plan.out_tile), BF16),
        ((chips - 1, tiles, block, plan.out_tile), BF16),
        ((chips - 1, tiles, block, plan.out_tile), BF16),
        ((block, depth), BF16),
    ]
    pieces = plan.pieces
    semaphores = [
        (13,), (1,), (chips - 1, pieces), (1,), (chips,),
        (1,), (1,), (1,), (1,), (1,), (1,), (1,), (1,),
        (1,), (1,), (1,), (1,), (units,), (fold,), (1,), (1,), (2,), (2,),
        (1,), ((chips - 1) * tiles + 1,), (1,), (chips - 1, tiles), (1,),
    ]
    return pl.pallas_call(
        functools.partial(layer_kernel, plan),
        in_specs=[hbm, hbm, vmem, vmem, hbm, hbm, hbm, vmem, hbm, hbm, hbm, hbm, vmem, hbm, hbm, hbm, hbm, vmem, hbm],
        out_specs=hbm,
        out_shape=jax.ShapeDtypeStruct(latent.shape, BF16),
        scratch_shapes=[pltpu.VMEM(shape, kind) for shape, kind in scratch]
        + [pltpu.SemaphoreType.DMA(shape) for shape in semaphores],
        compiler_params=pltpu.CompilerParams(
            collective_id=0, has_side_effects=True, vmem_limit_bytes=VMEM_BYTES
        ),
        name="layer",
    )(
        latent, context, condition.reshape(1, -1), context_condition.reshape(1, -1),
        shift_weight, scale_weight, gate_weight, norm_gain.reshape(1, -1),
        decay_down, decay_up, rate_down, rate_up, head_bias,
        query_weight, key_weight, value_weight, branch_weight, group_gain.reshape(1, -1), out_weight,
    )


def solution(mesh):
    placed = (
        P(("sp", "tp"), None),
        P("sp", None),
        P("sp"),
        P("sp"),
        P("sp", "tp"),
        P("sp", "tp"),
        P("sp", "tp"),
        P(),
        P(),
        P(None, "tp"),
        P(),
        P(None, "tp"),
        P(None, "tp"),
        P(None, "tp"),
        P(None, "tp"),
        P(None, "tp"),
        P(None, "tp"),
        P("tp"),
        P("tp", None),
    )
    return jax.shard_map(
        on_device, mesh=mesh, in_specs=placed, out_specs=P(("sp", "tp"), None), check_vma=False
    )
```

time: 65 us -> 55.6 us (0.86)
  Pallas kernels: 63.1 us -> 53.7 us
    pallas_call x1, Pallas kernels: 63.1 us -> 53.7 us  [on_device(): pl.pallas_call(functools.partial(layer_kernel, plan), in_specs=[hbm, hbm,...]
where the time goes in v2:
time: 55.6 us; the launch traced here: 55.3 us
  Pallas kernels  53.7 us (97%)
  local copies, waits for them, and re-layouts  1.67 us (3%)
    pallas_call x1, Pallas kernels, on_device(): pl.pallas_call(functools.partial(layer_kernel, plan), in_specs=[hbm, hbm,...  53.7 us
    unnamed x1, local copies, waits for them, and re-layouts  1.67 us

profile of v2, /device:TPU:0, one launch (start us, length us, event | category | flops | bytes accessed | tf_op | source)
XLA Modules:
  0.0 55.3 jit_solution(16207605572561670185)
XLA Ops:
  0.0 53.7 %layer.1 = bf16[32,4096]{1,0:T(8,128)(2,1)} custom-call(bf16[32,4096]{1,0:T(8,128)(2,1)} %latent_hbm.1, bf16[32,4096]{1,0:T(8,128)(2,1)} %context_hbm.1, f32[1,512]{1,0:T(1,128)} %bitcast.6, f32[1,512]{1,0:T(1,128)} %bitcast.7, bf16[512,1024]{1,0:T(8,128)(2,1)} %shift_hbm.1, bf16[512,1024]{1,0:T(8,128)(2,1)} %scale_hbm.1, bf16[512,1024]{1,0:T(8,128)(2,1)} %gate_hbm.1, ...), custom_call_target="tpu_custom_call" | custom-call | tf_op jit(solution)/shard_map/layer/pallas_call | solution.py:861
  53.7 1.7 %copy.21 = bf16[32,4096]{1,0:T(8,128)(2,1)} copy(bf16[32,4096]{1,0:T(8,128)(2,1)} %layer.1) | data formatting | bytes 524288

commit v3 on v2

--- a/solution.py
+++ b/solution.py
@@ -129,7 +129,7 @@
         both = mmt(item["es"], above(item["wg"], item["kg"]))
         item["coupling"] = jnp.where(strict, both[:, :width], 0.0)
         item["feed"] = jnp.where(strict, both[:, width:], 0.0)
-        tail = jnp.exp(total - cum)
+        tail = jnp.exp(total) * growth
         item["wt"], item["kt"] = (write * tail).astype(BF16), (k * tail).astype(BF16)
         item["diagonal"] = unit * jnp.exp(total)
         work.append(item)
@@ -202,17 +202,17 @@
 
 def layer_kernel(
     plan,
-    latent_hbm, context_hbm, condition_ref, context_condition_ref,
-    shift_hbm, scale_hbm, gate_hbm, norm_gain_ref,
-    decay_down_hbm, decay_up_hbm, rate_down_hbm, rate_up_hbm, bias_ref,
-    query_hbm, key_hbm, value_hbm, branch_hbm, group_gain_ref, out_hbm,
+    latent_hbm, context_hbm, condition_hbm, context_condition_hbm,
+    shift_hbm, scale_hbm, gate_hbm, norm_gain_hbm,
+    decay_down_hbm, decay_up_hbm, rate_down_hbm, rate_up_hbm, bias_hbm,
+    query_hbm, key_hbm, value_hbm, branch_hbm, group_gain_hbm, out_hbm,
     updated_hbm,
-    rows_v, context_v, wmod_v, wdown_v, wup_v, wbig_v,
+    condition_v, norm_gain_ref, bias_ref, group_gain_ref, rows_v, context_v, wmod_v, wdown_v, wup_v, wbig_v,
     parts_v, part_in_v, vectors_v, gate_part_v, gate_in_v, gate_all_v, mod_v, inverse_v, normed_v,
     key_v, value_v, decay_v, rate_v, query_v, branch_v, bias_v,
     feature_out_v, feature_in_v, maps_out_v, maps_in_v, reads_q_v, base_v,
     saved_v, cum_v, first_v, transfer_v, constant_v,
-    state_out_v, state_in_v, turn_out_v, turn_in_v, entry_out_v, entry_in_v, mixed_v,
+    prefix_v, state_out_v, state_in_v, turn_out_v, turn_in_v, entry_out_v, entry_in_v, mixed_v,
     partial_v, pair_v, cross_out_v, cross_in_v, mixer_v,
     local_sem, row_s, row_r, relay_s, relay_r, part_s, part_r, vec_s, vec_r, gp_s, gp_r, gv_s, gv_r,
     feat_s, feat_r, map_s, map_r, st_s, st_r, turn_s, turn_r, ent_s, ent_r, pair_s, pair_r, cross_s, cross_r, store_sem,
@@ -231,20 +231,15 @@
         copy.start()
         fetches[name] = copy
 
-    fetch("shift", 0, shift_hbm, wmod_v.at[0])
-    fetch("scale", 1, scale_hbm, wmod_v.at[1])
-    fetch("gate", 2, gate_hbm, wmod_v.at[2])
-    fetch("latent", 3, latent_hbm, rows_v.at[me_tp])
-    fetch("context", 4, context_hbm, context_v)
-
     def settle(ref, semaphore):
         remote(ref, ref, semaphore, semaphore, sp=me_sp, tp=me_tp).wait_recv()
 
     peers = sorted(range(1, sp), key=lambda d: (abs(d - half), d))
 
     barrier = pltpu.get_barrier_semaphore()
-    everyone = [(a, b) for a in range(sp) for b in range(tp) if (a, b) != (0, 0)]
-    for a, b in everyone:
+    everyone = [(a, b) for a in (*peers, 0) for b in reversed(range(tp)) if (a, b) != (0, 0)]
+    greeted = [(a, b) for a, b in everyone if a == 0 or b == 0]
+    for a, b in greeted:
         pl.semaphore_signal(
             barrier,
             inc=1,
@@ -252,24 +247,27 @@
             device_id_type=MESH,
         )
 
-    line = lax.broadcasted_iota(jnp.int32, (8, condition_ref.shape[1]), 0)
-    values = jnp.where(line == 0, condition_ref[...], jnp.where(line == 1, context_condition_ref[...], 0.0))
+    fetch("condition", 10, condition_hbm, condition_v.at[0])
+    fetch("context_condition", 10, context_condition_hbm, condition_v.at[1])
+    fetch("shift", 0, shift_hbm, wmod_v.at[0])
+    fetch("scale", 1, scale_hbm, wmod_v.at[1])
+    fetch("latent", 3, latent_hbm, rows_v.at[me_tp])
+    fetch("context", 4, context_hbm, context_v)
+    fetch("norm_gain", 13, norm_gain_hbm, norm_gain_ref)
+    fetch("bias", 14, bias_hbm, bias_ref)
+    fetch("group_gain", 15, group_gain_hbm, group_gain_ref)
+
+    line = lax.broadcasted_iota(jnp.int32, (8, condition_v.shape[2]), 0)
+    settle(condition_v, local_sem.at[10])
+    values = jnp.where(line == 0, condition_v[0], jnp.where(line == 1, condition_v[1], 0.0))
     conditions = (values * jax.nn.sigmoid(values)).astype(BF16)
-    shares = []
-    for at, name in enumerate(("shift", "scale", "gate")):
+    for at, name in enumerate(("shift", "scale")):
         fetches[name].wait()
-        shares.append(mm(conditions, wmod_v[at])[0:2])
-    fetch("decay_down", 5, decay_down_hbm, wdown_v.at[:, 0 : decay_down_hbm.shape[1]])
-    fetch("rate_down", 5, rate_down_hbm, wdown_v.at[:, decay_down_hbm.shape[1] :])
-    fetch("key", 7, key_hbm, wbig_v.at[0])
-    fetch("value", 8, value_hbm, wbig_v.at[1])
-    for j in range(plan.owners):
-        c = slice(j * plan.chunk, (j + 1) * plan.chunk)
-        parts_v[j, 0:2] = shares[0][:, c]
-        parts_v[j, 2:4] = shares[1][:, c]
-        gate_part_v[j] = shares[2][0:1, c]
-
-    pl.semaphore_wait(barrier, len(everyone))
+        share = mm(conditions, wmod_v[at])[0:2]
+        for j in range(plan.owners):
+            parts_v[j, 2 * at : 2 * at + 2] = share[:, j * plan.chunk : (j + 1) * plan.chunk]
+
+    pl.semaphore_wait(barrier, len(greeted))
 
     def part_copy(d):
         peer = lax.rem(me_sp + d, sp)
@@ -289,7 +287,7 @@
         else:
             pl.when(at < plan.owners)(body)
 
-    for d in range(1, sp):
+    for d in peers:
         peer = lax.rem(me_sp + d, sp)
         when_owner(peer, lambda d=d: part_copy(d)[1].start())
 
@@ -317,8 +315,11 @@
         copy.start()
     for i in range(plan.pieces):
         relay_copies[i].start()
-    for d in range(1, sp):
-        when_owner(lax.rem(me_sp + d, sp), lambda d=d: gate_copy(d).start())
+    fetch("gate", 2, gate_hbm, wmod_v.at[2])
+    fetch("decay_down", 5, decay_down_hbm, wdown_v.at[:, 0 : decay_down_hbm.shape[1]])
+    fetch("rate_down", 5, rate_down_hbm, wdown_v.at[:, decay_down_hbm.shape[1] :])
+    fetch("key", 7, key_hbm, wbig_v.at[0])
+    fetch("value", 8, value_hbm, wbig_v.at[1])
 
     my_slot = me_tp * plan.owners + me_sp
     vector_copies = [
@@ -345,6 +346,13 @@
     fetch("query", 11, query_hbm, wbig_v.at[2])
     fetch("branch", 12, branch_hbm, wbig_v.at[3])
 
+    fetches["gate"].wait()
+    share = mm(conditions, wmod_v[2])[0:1]
+    for j in range(plan.owners):
+        gate_part_v[j] = share[:, j * plan.chunk : (j + 1) * plan.chunk]
+    for d in peers:
+        when_owner(lax.rem(me_sp + d, sp), lambda d=d: gate_copy(d).start())
+
     def inverse_of(x):
         x = x.astype(F32)
         mean = jnp.sum(x * x, axis=-1, keepdims=True) * (1.0 / depth)
@@ -358,6 +366,8 @@
         for at in range(0, block, 16):
             inverse_v[(slot * block + at) // 16] = inverse_of(rows_v[slot, at : at + 16])
 
+    for name in ("norm_gain", "bias", "group_gain"):
+        fetches[name].wait()
     for p in range(packs):
         bias_v[p] = bias_ref[:, p * width : (p + 1) * width]
     block_inverse(me_tp)
@@ -397,7 +407,7 @@
 
     per = block // 16
 
-    @pl.loop(0, plan.rows // 16)
+    @pl.loop(0, plan.rows // 16, unroll=2)
     def _(g):
         slot, at = g // per, lax.rem(g, per) * 16
         modulate(lambda c: rows_v[slot, pl.ds(pl.multiple_of(at, 16), 16), c], g, 0)
@@ -408,13 +418,12 @@
     rank = decay_down_hbm.shape[1]
     settle(wdown_v, local_sem.at[5])
     settle(wup_v, local_sem.at[9])
+    fetches["key"].wait()
+    fetches["value"].wait()
     low = sum(
         jnp.dot(normed_v[:, c], wdown_v[c], preferred_element_type=F32)
         for c in (slice(0, depth // 2), slice(depth // 2, depth))
     )
-    decay_low = jnp.tanh(low[:, :rank]).astype(BF16)
-    rate_low = low[:, rank:].astype(BF16)
-
     gate_copies = [
         remote(
             gate_all_v.at[my_slot], gate_all_v.at[my_slot], gv_s.at[0], gv_r.at[0],
@@ -440,6 +449,32 @@
             if kind is not None:
                 feature_out_v[at // width + p, kind] = piece[plan.rows :]
 
+    def project(which, rows, target, kind, tiles):
+        for at in tiles:
+            found = jnp.dot(
+                normed_v[0:rows], wbig_v[which, :, at : at + plan.tile], preferred_element_type=F32
+            )
+            spread(found, at, target, kind)
+
+    def pack_of(d):
+        return (d * units) // 2
+
+    def feature_part(at, i):
+        return at.at[(pl.ds(2, 2), pl.ds(0, 1), pl.ds(1, 1))[i]]
+
+    def feature_copy(d, i):
+        peer = lax.rem(me_sp + d, sp)
+        return remote(
+            feature_part(feature_out_v.at[pack_of(peer)], i), feature_part(feature_in_v.at[me_sp], i),
+            feat_s.at[0], feat_r.at[0], sp=peer, tp=me_tp,
+        )
+
+    everything = plan.rows + plan.context_rows
+    tiles = list(range(0, local, plan.tile))
+    project(0, everything, key_v, 0, tiles[:1])
+    decay_low = jnp.tanh(low[:, :rank]).astype(BF16)
+    rate_low = low[:, rank:].astype(BF16)
+
     for name, lhs, which, target, kind in (
         ("decay_up", decay_low, 0, decay_v, 2),
         ("rate_up", rate_low, 1, rate_v, 3),
@@ -447,37 +482,14 @@
         for at in range(0, local, plan.tile):
             found = jnp.dot(lhs, wup_v[which, :, at : at + plan.tile], preferred_element_type=F32)
             spread(found, at, target, kind)
-
-    def project(name, which, rows, target, kind):
-        fetches[name].wait()
-        for at in range(0, local, plan.tile):
-            found = jnp.dot(
-                normed_v[0:rows], wbig_v[which, :, at : at + plan.tile], preferred_element_type=F32
-            )
-            spread(found, at, target, kind)
-
-    def pack_of(d):
-        return (d * units) // 2
-
-    def feature_part(at, i):
-        return at.at[(pl.ds(2, 2), pl.ds(0, 1), pl.ds(1, 1))[i]]
-
-    def feature_copy(d, i):
-        peer = lax.rem(me_sp + d, sp)
-        return remote(
-            feature_part(feature_out_v.at[pack_of(peer)], i), feature_part(feature_in_v.at[me_sp], i),
-            feat_s.at[0], feat_r.at[0], sp=peer, tp=me_tp,
-        )
-
-    everything = plan.rows + plan.context_rows
     for d in peers:
         feature_copy(d, 0).start()
-    project("key", 0, everything, key_v, 0)
+    project(0, everything, key_v, 0, tiles[1:])
     for d in peers:
         feature_copy(d, 1).start()
     for j in range(plan.out_tiles):
         fetch("out", 6, out_hbm.at[:, j * local : (j + 1) * local], wbig_v.at[0, j * local : (j + 1) * local])
-    project("value", 1, everything, value_v, 1)
+    project(1, everything, value_v, 1, tiles)
     for d in peers:
         feature_copy(d, 2).start()
     feature_in_v[me_sp] = feature_out_v[pack_of(me_sp)]
@@ -575,7 +587,8 @@
         def _(u=u, slot=slot):
             state_in_v[slot] = state_out_v[u]
 
-    project("query", 2, plan.rows, query_v, None)
+    fetches["query"].wait()
+    project(2, plan.rows, query_v, None, tiles)
 
     def latent_queries(s):
         jobs = []
@@ -615,31 +628,42 @@
             ent_s.at[stage], ent_r.at[stage], sp=side * half + at, tp=me_tp,
         )
 
+    def place(way, step):
+        return jnp.where(way == 0, step, half - 1 - step)
+
+    def compose_maps(way):
+        for i in range(fold):
+            found = maps_in_v[place(way, 0), i, way]
+            both = jnp.concatenate([found[0].astype(F32), found[1].astype(F32)], axis=0)
+            prefix_v[way, i, 0] = both.astype(BF16)
+            for step in range(1, half):
+                found = maps_in_v[place(way, step), i, way]
+                both = mm(both, stack_heads(found[0]))
+                both = jnp.concatenate([both[:HEAD_DIM], both[HEAD_DIM:] + found[1].astype(F32)], axis=0)
+                prefix_v[way, i, step] = both.astype(BF16)
+
+    def moved(way, i, step, state):
+        found = prefix_v[way, i, step]
+        return advance(state, stack_heads(found[:HEAD_DIM]), found[HEAD_DIM:].astype(F32))
+
     def fold_maps(stage, way, start):
         states = [start[i].astype(F32) for i in range(fold)]
-        for step in range(half):
-            at = jnp.where(way == 0, step, half - 1 - step)
+        for i in range(fold):
+            entry_out_v[stage, place(way, 0), i] = start[i]
+        for step in range(1, half):
             for i in range(fold):
-                entry_out_v[stage, at, i] = states[i].astype(BF16)
-
-            @pl.when(at != index)
-            def _(at=at):
-                entry_copy(stage, way, at).start()
-
-            if stage == 0 or step < half - 1:
-                for i in range(fold):
-                    states[i] = advance(
-                        states[i], stack_heads(maps_in_v[at, i, way, 0]), maps_in_v[at, i, way, 1].astype(F32)
-                    )
+                entry_out_v[stage, place(way, step), i] = moved(way, i, step - 1, states[i]).astype(BF16)
+        for d in range(1, half):
+            entry_copy(stage, way, lax.rem(index + d, half)).start()
         for i in range(fold):
             entry_in_v[way, index * fold + i] = entry_out_v[stage, index, i]
-        return states
 
     def entries_arrived(stage, way):
         settle(entry_in_v.at[way, pl.ds(0, (half - 1) * fold)], ent_r.at[stage])
 
-    pl.loop(0, groups)(latent_queries)
     settle(maps_in_v.at[pl.ds(0, half - 1)], map_r.at[0])
+    for way in (0, 1):
+        compose_maps(way)
     for i in range(fold):
         p = index * fold + i
 
@@ -649,15 +673,17 @@
                 state_out_v.at[0], state_in_v.at[i], st_s.at[0], st_r.at[i], sp=me_sp, tp=me_tp
             ).wait_recv()
 
-    states = fold_maps(0, side, state_in_v)
     for i in range(fold):
-        turn_out_v[i] = states[i].astype(BF16)
+        turn_out_v[i] = moved(side, i, half - 1, state_in_v[i].astype(F32)).astype(BF16)
     turn = remote(
         turn_out_v, turn_in_v, turn_s.at[0], turn_r.at[0], sp=(1 - side) * half + index, tp=me_tp
     )
     turn.start()
-
-    project("branch", 3, plan.rows, branch_v, None)
+    fold_maps(0, side, state_in_v)
+    pl.loop(0, groups)(latent_queries)
+
+    fetches["branch"].wait()
+    project(3, plan.rows, branch_v, None, tiles)
     turn.wait_recv()
     fold_maps(1, 1 - side, turn_in_v)
 
@@ -802,9 +828,12 @@
     rows, crows, tiles = plan.rows, plan.context_rows, plan.out_tiles
     half, fold, blocks = plan.half, plan.fold, rows // BLOCK
     rank = decay_down.shape[1]
-    vmem = pl.BlockSpec(memory_space=pltpu.VMEM)
     hbm = pl.BlockSpec(memory_space=pltpu.HBM)
     scratch = [
+        ((2, 1, condition.shape[0]), F32),
+        ((1, depth), F32),
+        ((2, local), F32),
+        ((1, local), F32),
         ((tp, block, depth), BF16),
         ((crows, depth), BF16),
         ((3, *shift_weight.shape), BF16),
@@ -838,6 +867,7 @@
         ((packs, 2, blocks, 2 * width, width), BF16),
         ((plan.context_blocks, width, width), BF16),
         ((plan.context_blocks, HEAD_DIM, width), F32),
+        ((2, fold, half, 2 * HEAD_DIM, width), BF16),
         ((units, HEAD_DIM, width), BF16),
         ((fold, HEAD_DIM, width), BF16),
         ((fold, HEAD_DIM, width), BF16),
@@ -853,14 +883,14 @@
     ]
     pieces = plan.pieces
     semaphores = [
-        (13,), (1,), (chips - 1, pieces), (1,), (chips,),
+        (16,), (1,), (chips - 1, pieces), (1,), (chips,),
         (1,), (1,), (1,), (1,), (1,), (1,), (1,), (1,),
         (1,), (1,), (1,), (1,), (units,), (fold,), (1,), (1,), (2,), (2,),
         (1,), ((chips - 1) * tiles + 1,), (1,), (chips - 1, tiles), (1,),
     ]
     return pl.pallas_call(
         functools.partial(layer_kernel, plan),
-        in_specs=[hbm, hbm, vmem, vmem, hbm, hbm, hbm, vmem, hbm, hbm, hbm, hbm, vmem, hbm, hbm, hbm, hbm, vmem, hbm],
+        in_specs=[hbm] * 19,
         out_specs=hbm,
         out_shape=jax.ShapeDtypeStruct(latent.shape, BF16),
         scratch_shapes=[pltpu.VMEM(shape, kind) for shape, kind in scratch]

time: 55.6 us -> 52 us (0.935)
  Pallas kernels: 53.7 us -> 50.1 us
    pallas_call x1, Pallas kernels: 53.7 us -> 50.1 us  [on_device(): pl.pallas_call(functools.partial(layer_kernel, plan), in_specs=[hbm] * 19...]
where the time goes in v3:
time: 52 us; the launch traced here: 51.8 us
  Pallas kernels  50.1 us (96%)
  local copies, waits for them, and re-layouts  1.67 us (3%)
    pallas_call x1, Pallas kernels, on_device(): pl.pallas_call(functools.partial(layer_kernel, plan), in_specs=[hbm] * 19...  50.1 us
    unnamed x1, local copies, waits for them, and re-layouts  1.67 us

profile of v3, /device:TPU:0, one launch (start us, length us, event | category | flops | bytes accessed | tf_op | source)
XLA Modules:
  0.0 51.8 jit_solution(735012729231249836)
XLA Ops:
  0.0 50.1 %layer.1 = bf16[32,4096]{1,0:T(8,128)(2,1)} custom-call(bf16[32,4096]{1,0:T(8,128)(2,1)} %latent_hbm.1, bf16[32,4096]{1,0:T(8,128)(2,1)} %context_hbm.1, f32[1,512]{1,0:T(1,128)} %bitcast.6, f32[1,512]{1,0:T(1,128)} %bitcast.7, bf16[512,1024]{1,0:T(8,128)(2,1)} %shift_hbm.1, bf16[512,1024]{1,0:T(8,128)(2,1)} %scale_hbm.1, bf16[512,1024]{1,0:T(8,128)(2,1)} %gate_hbm.1, ...), custom_call_target="tpu_custom_call" | custom-call | tf_op jit(solution)/shard_map/layer/pallas_call | solution.py:891
  50.1 1.7 %copy.21 = bf16[32,4096]{1,0:T(8,128)(2,1)} copy(bf16[32,4096]{1,0:T(8,128)(2,1)} %layer.1) | data formatting | bytes 524288

commit v4 on v3

--- a/solution.py
+++ b/solution.py
@@ -682,10 +682,10 @@
     fold_maps(0, side, state_in_v)
     pl.loop(0, groups)(latent_queries)
 
+    turn.wait_recv()
+    fold_maps(1, 1 - side, turn_in_v)
     fetches["branch"].wait()
     project(3, plan.rows, branch_v, None, tiles)
-    turn.wait_recv()
-    fold_maps(1, 1 - side, turn_in_v)
 
     entries_arrived(0, side)
     for p in range(packs):

time: 52 us -> 51.4 us (0.988)
    pallas_call x1, Pallas kernels: 50.1 us -> 49.6 us  [on_device(): pl.pallas_call(functools.partial(layer_kernel, plan), in_specs=[hbm] * 19...]
where the time goes in v4:
time: 51.4 us; the launch traced here: 51.2 us
  Pallas kernels  49.6 us (96%)
  local copies, waits for them, and re-layouts  1.67 us (3%)
    pallas_call x1, Pallas kernels, on_device(): pl.pallas_call(functools.partial(layer_kernel, plan), in_specs=[hbm] * 19...  49.6 us
    unnamed x1, local copies, waits for them, and re-layouts  1.67 us

profile of v4, /device:TPU:0, one launch (start us, length us, event | category | flops | bytes accessed | tf_op | source)
XLA Modules:
  0.0 51.2 jit_solution(6629493416062460896)
XLA Ops:
  0.0 49.6 %layer.1 = bf16[32,4096]{1,0:T(8,128)(2,1)} custom-call(bf16[32,4096]{1,0:T(8,128)(2,1)} %latent_hbm.1, bf16[32,4096]{1,0:T(8,128)(2,1)} %context_hbm.1, f32[1,512]{1,0:T(1,128)} %bitcast.6, f32[1,512]{1,0:T(1,128)} %bitcast.7, bf16[512,1024]{1,0:T(8,128)(2,1)} %shift_hbm.1, bf16[512,1024]{1,0:T(8,128)(2,1)} %scale_hbm.1, bf16[512,1024]{1,0:T(8,128)(2,1)} %gate_hbm.1, ...), custom_call_target="tpu_custom_call" | custom-call | tf_op jit(solution)/shard_map/layer/pallas_call | solution.py:891
  49.6 1.7 %copy.21 = bf16[32,4096]{1,0:T(8,128)(2,1)} copy(bf16[32,4096]{1,0:T(8,128)(2,1)} %layer.1) | data formatting | bytes 524288
